TPU v7x, 32 devices: a whole 2x2x4 slice. The times are simulated.
32 devices in a mesh: sp: 8 (over z, y), tp: 4 (over x, core).
Axes of the slice: x: 2, y: 2, z: 4, core: 2. Of those that a mesh axis runs over, the one named last changes fastest.
Arguments:
- activations: bfloat16 [6144, 2048], P(('sp', 'tp')), may hold values from -6 to 6
- in_gain: float32 [2048], replicated, may hold values from 0.1 to 1.9
- w_pool_in: bfloat16 [2048, 1024], P(None, 'tp'), may hold values from -0.125 to 0.125
- pool_gain: float32 [1024], P('tp'), may hold values from 0.1 to 1.9
- w_qlat: bfloat16 [2048, 768], P(None, 'tp'), may hold values from -0.125 to 0.125
- w_kvlat: bfloat16 [2048, 512], P(None, 'tp'), may hold values from -0.125 to 0.125
- w_krope: bfloat16 [2048, 32], replicated, may hold values from -0.125 to 0.125
- qlat_gain: float32 [768], replicated, may hold values from 0.1 to 1.9
- kvlat_gain: float32 [512], replicated, may hold values from 0.1 to 1.9
- w_qup: bfloat16 [768, 1536], P(None, 'tp'), may hold values from -0.21875 to 0.21875
- w_kup: bfloat16 [512, 1024], P(None, 'tp'), may hold values from -0.25 to 0.25
- w_vup: bfloat16 [512, 1024], P(None, 'tp'), may hold values from -0.25 to 0.25
- qhead_gain: float32 [96], replicated, may hold values from 1.1 to 1.9
- khead_gain: float32 [96], replicated, may hold values from 1.1 to 1.9
- w_out_pool: bfloat16 [1024, 2048], P('tp'), may hold values from -0.1875 to 0.1875
- w_out_attn: bfloat16 [1024, 2048], P('tp'), may hold values from -0.75 to 0.75
Outputs:
- mixed: bfloat16 [6144, 2048], P(('sp', 'tp'))
All inputs are finite; a program needn't handle non-finite values.
Results may differ from a plain program's by a relative error of at most 0.025.
Values may be sent and summed in bfloat16 or wider, within the bound.
A program may use at most 128 MiB of HBM per device.

v0:
```python
import math

import jax
import jax.numpy as jnp
from jax import lax
from jax.sharding import PartitionSpec as P

GROUP = 256
NOPE = 64
ROPE = 32
VDIM = 64
QLAT = 768
KVLAT = 512


norm_eps = 1e-06
rope_theta = 10000.0
rim_depth = 15
block_rows = 512


def from_behind(block, axis, distance):
    devices = range(lax.axis_size(axis))
    route = [(i - distance, i) for i in devices if i - distance in devices]
    return lax.ppermute(block, axis, route)


def row_norm(source, norm_gain):
    as_float = source.astype(jnp.float32)
    factor = lax.rsqrt(jnp.mean(as_float * as_float, axis=-1, keepdims=True) + norm_eps)
    return as_float * factor * norm_gain


def rotate(head_rows, positions):
    half_rope = ROPE // 2
    frequency = rope_theta ** (-jnp.arange(0, ROPE, 2, dtype=jnp.float32) / ROPE)
    angles = positions.astype(jnp.float32)[:, None] * frequency[None, :]
    cosine = jnp.cos(angles)[:, None, :]
    sine_part = jnp.sin(angles)[:, None, :]
    plain_part = head_rows[..., :NOPE]
    lower_half = head_rows[..., NOPE : NOPE + half_rope]
    upper_half = head_rows[..., NOPE + half_rope :]
    return jnp.concatenate(
        [
            plain_part,
            lower_half * cosine - upper_half * sine_part,
            upper_half * cosine + lower_half * sine_part,
        ],
        axis=-1,
    )


def pool_mix(extended, positions, channel_start):
    row_count = positions.shape[0]
    width = extended.shape[1]
    channel = channel_start + jnp.arange(width, dtype=jnp.int32)
    window = jnp.left_shift(jnp.int32(2), channel // GROUP)
    as_float = extended.astype(jnp.float32)
    window_sum = jnp.zeros((row_count, width), jnp.float32)
    for lag_index in range(rim_depth + 1):
        lagged = as_float[rim_depth - lag_index : rim_depth - lag_index + row_count]
        window_sum = window_sum + jnp.where(lag_index < window[None, :], lagged, 0.0)
    divisor = jnp.minimum(positions[:, None] + 1, window[None, :]).astype(jnp.float32)
    return window_sum / divisor - as_float[rim_depth:]


def make_queries(q_normed, w_qup, norm_gain, positions):
    row_count = q_normed.shape[0]
    head_count = w_qup.shape[1] // (NOPE + ROPE)
    query_raw = jnp.dot(q_normed, w_qup, preferred_element_type=jnp.float32).astype(jnp.bfloat16)
    query_raw = query_raw.reshape(row_count, head_count, NOPE + ROPE)
    return rotate(row_norm(query_raw, norm_gain), positions).astype(jnp.bfloat16)


def plain_parts(kv_rows, w_kup, w_vup):
    key_plain = jnp.dot(kv_rows, w_kup, preferred_element_type=jnp.float32).astype(jnp.bfloat16)
    value_rows = jnp.dot(kv_rows, w_vup, preferred_element_type=jnp.float32).astype(jnp.bfloat16)
    return (key_plain, value_rows)


def finish_keys(key_plain, rope_rows, norm_gain, positions):
    row_count = key_plain.shape[0]
    head_count = key_plain.shape[1] // NOPE
    key_plain = key_plain.reshape(row_count, head_count, NOPE)
    shared = jnp.broadcast_to(rope_rows[:, None, :], (row_count, head_count, ROPE))
    joined = jnp.concatenate([key_plain, shared], axis=-1)
    key_rows = rotate(row_norm(joined, norm_gain), positions).astype(jnp.bfloat16)
    return key_rows.reshape(row_count, head_count * (NOPE + ROPE))


def update(state_pair, queries, query_pos, key_rows, value_rows, key_pos):
    numerator, denominator = state_pair
    head_count = queries.shape[1]
    key_rows = key_rows.reshape(key_rows.shape[0], head_count, NOPE + ROPE)
    value_rows = value_rows.reshape(value_rows.shape[0], head_count, VDIM)
    scores = jnp.einsum("qhd,khd->hqk", queries, key_rows, preferred_element_type=jnp.float32)
    scores = scores * (NOPE + ROPE) ** (-0.5)
    weights = jnp.where(key_pos[None, None, :] <= query_pos[None, :, None], jnp.exp(scores), 0.0)
    denominator = denominator + jnp.sum(weights, axis=-1)
    numerator = numerator + jnp.einsum(
        "hqk,khd->qhd", weights.astype(jnp.bfloat16), value_rows, preferred_element_type=jnp.float32
    )
    return (numerator, denominator)


def sweep(state_pair, pieces, expand, queries, query_pos):
    shard_rows = queries.shape[0]
    piece_rows = pieces[0].shape[0]
    block_size = shard_rows * math.gcd(piece_rows // shard_rows, max(1, block_rows // shard_rows))

    def advance(block_index, current):
        offset = block_index * block_size

        def accumulate(inner):
            chosen = tuple(
                (lax.dynamic_slice_in_dim(member, offset, block_size, 0) for member in pieces)
            )
            key_pos = offset + jnp.arange(block_size, dtype=jnp.int32)
            key_rows, value_rows = expand(chosen, key_pos)
            return update(inner, queries, query_pos, key_rows, value_rows, key_pos)

        def unchanged(inner):
            return inner

        return lax.cond(offset <= query_pos[-1], accumulate, unchanged, current)

    return lax.fori_loop(0, piece_rows // block_size, advance, state_pair)


def local(
    activations,
    in_gain,
    w_pool_in,
    pool_gain,
    w_qlat,
    w_kvlat,
    w_krope,
    qlat_gain,
    kvlat_gain,
    w_qup,
    w_kup,
    w_vup,
    qhead_gain,
    khead_gain,
    w_out_pool,
    w_out_attn,
):
    own_input = lax.all_gather(activations, "tp", axis=0, tiled=True)
    row_count = own_input.shape[0]
    positions = lax.axis_index("sp") * row_count + jnp.arange(row_count, dtype=jnp.int32)
    normed = row_norm(own_input, in_gain).astype(jnp.bfloat16)
    pool_in = jnp.dot(normed, w_pool_in, preferred_element_type=jnp.float32).astype(jnp.bfloat16)
    prev_rows = from_behind(pool_in[row_count - rim_depth :], "sp", 1)
    extended = jnp.concatenate([prev_rows, pool_in], axis=0)
    channel_start = lax.axis_index("tp") * pool_in.shape[1]
    pool_out = (pool_mix(extended, positions, channel_start) * pool_gain).astype(jnp.bfloat16)
    q_part = jnp.dot(normed, w_qlat, preferred_element_type=jnp.float32).astype(jnp.bfloat16)
    kv_part = jnp.dot(normed, w_kvlat, preferred_element_type=jnp.float32).astype(jnp.bfloat16)
    rope_key = jnp.dot(normed, w_krope, preferred_element_type=jnp.float32).astype(jnp.bfloat16)
    tp_index = lax.axis_index("tp")
    q_width = q_part.shape[1]
    kv_width = kv_part.shape[1]
    q_float = q_part.astype(jnp.float32)
    kv_float = kv_part.astype(jnp.float32)
    q_squares, kv_squares = lax.psum(
        (jnp.sum(q_float * q_float, axis=1), jnp.sum(kv_float * kv_float, axis=1)), "tp"
    )
    q_gain = lax.dynamic_slice_in_dim(qlat_gain, tp_index * q_width, q_width)
    kv_gain = lax.dynamic_slice_in_dim(kvlat_gain, tp_index * kv_width, kv_width)
    q_scaled = q_float * lax.rsqrt(q_squares / QLAT + norm_eps)[:, None] * q_gain
    kv_scaled = kv_float * lax.rsqrt(kv_squares / KVLAT + norm_eps)[:, None] * kv_gain
    q_normed, kv_normed = (
        lax.all_gather(q_scaled.astype(jnp.bfloat16), "tp", axis=1, tiled=True),
        lax.all_gather(kv_scaled.astype(jnp.bfloat16), "tp", axis=1, tiled=True),
    )
    queries = make_queries(q_normed, w_qup, qhead_gain, positions)
    head_count = queries.shape[1]
    start_pair = (
        jnp.zeros((row_count, head_count, VDIM), jnp.float32),
        jnp.zeros((head_count, row_count), jnp.float32),
    )
    key_plain, value_rows = plain_parts(kv_normed, w_kup, w_vup)

    def expand_plain(chosen, key_pos):
        return (finish_keys(chosen[0], chosen[2], khead_gain, key_pos), chosen[1])

    numerator, denominator = sweep(
        start_pair,
        (
            lax.all_gather(key_plain, "sp", axis=0, tiled=True),
            lax.all_gather(value_rows, "sp", axis=0, tiled=True),
            lax.all_gather(rope_key, "sp", axis=0, tiled=True),
        ),
        expand_plain,
        queries,
        positions,
    )
    attended = (numerator / jnp.transpose(denominator)[:, :, None]).astype(jnp.bfloat16)
    attended = attended.reshape(row_count, head_count * VDIM)
    term = jnp.dot(pool_out, w_out_pool, preferred_element_type=jnp.float32)
    return lax.psum_scatter(
        (term + jnp.dot(attended, w_out_attn, preferred_element_type=jnp.float32)).astype(
            jnp.bfloat16
        ),
        "tp",
        scatter_dimension=0,
        tiled=True,
    )


def solution(mesh):
    placed = (
        P(("sp", "tp"), None),
        P(),
        P(None, "tp"),
        P("tp"),
        P(None, "tp"),
        P(None, "tp"),
        P(),
        P(),
        P(),
        P(None, "tp"),
        P(None, "tp"),
        P(None, "tp"),
        P(),
        P(),
        P("tp", None),
        P("tp", None),
    )
    return jax.shard_map(
        local, mesh=mesh, in_specs=placed, out_specs=P(("sp", "tp"), None), check_vma=False
    )
```

profile of v0, /device:TPU:30, one launch (start us, length us, event | category | flops | bytes accessed | tf_op | source)
XLA Modules:
  0.0 316.1 jit_solution(7002376077708482121)
XLA Ops:
  8.1 29.4 %all-gather.5.cloned.1.call-done = bf16[768,2048]{1,0:T(8,128)(2,1)} async-done(((bf16[192,2048]{1,0:T(8,128)(2,1)}), bf16[768,2048]{1,0:T(8,128)(2,1)}) %all-gather.5.cloned.1.call-update) | async-done | bytes 3145744 | tf_op jit(solution)/shard_map/all_gather | solution.py:148
  37.4 2.7 fusion.23
  44.2 7.1 %all-reduce = (f32[768]{0:T(1024)S(1)}, f32[768]{0:T(1024)S(1)}) all-reduce(f32[768]{0:T(1024)S(1)} %get-tuple-element.242, f32[768]{0:T(1024)S(1)} %get-tuple-element.244), channel_id=1, replica_groups=mesh['sp'=8,'tp'=4] {'tp'}, use_global_device_ids=true, to_apply=%region_2.3 | all-reduce | flops 1536 | bytes 12288 | tf_op jit(solution)/shard_map/psum | solution.py:165
  53.1 7.7 %all_gather.19 = bf16[768,512]{0,1:T(8,128)(2,1)S(1)} all-gather(bf16[768,128]{0,1:T(8,128)(2,1)S(1)} %multiply_convert_fusion.1), channel_id=1, replica_groups=mesh['sp'=8,'tp'=4] {'tp'}, dimensions={1}, use_global_device_ids=true | all-gather | bytes 983040 | tf_op jit(solution)/shard_map/all_gather | solution.py:174
  62.1 2.1 convolution_convert_fusion.1
  64.8 3.1 convolution_convert_fusion.3
  70.2 32.6 %all_gather.22 = bf16[6144,32]{0,1:T(8,128)(2,1)S(1)} all-gather(bf16[768,32]{0,1:T(8,128)(2,1)S(1)} %convolution_convert_fusion.6), channel_id=1, replica_groups=mesh['sp'=8,'tp'=4] {'sp'}, dimensions={0}, use_global_device_ids=true | all-gather | bytes 442368 | tf_op jit(solution)/shard_map/all_gather | solution.py:192
  102.9 5.2 %fusion.49 = f32[768,2048]{1,0:T(8,128)} fusion(bf16[256,2048]{1,0:T(8,128)(2,1)S(1)} %copy-done, f32[783,256]{1,0:T(8,128)S(1)} %maximum_convert_fusion, f32[256]{0:T(256)S(1)} %copy-done.15, s32[256]{0:T(256)S(1)} %fusion.69, s32[768]{0:T(1024)S(1)} %fusion.68, pred[256]{0:T(512)(128)(4,1)S(1)} %get-tuple-element.246, ...), kind=kOutput, calls=%fused_computation.95 | convolution fusion | flops 812580864 | bytes 19937280 | tf_op jit(solution)/shard_map/dot_general | solution.py:200
  111.5 21.2 %all-gather.7.cloned.1.call-done = bf16[6144,256]{1,0:T(8,128)(2,1)} async-done(((bf16[768,256]{1,0:T(8,128)(2,1)}), bf16[6144,256]{1,0:T(8,128)(2,1)}) %all-gather.7.cloned.1.call-update) | async-done | bytes 3145744 | tf_op jit(solution)/shard_map/all_gather | solution.py:191
  132.6 4.6 %copy.18 = bf16[6144,256]{0,1:T(8,128)(2,1)} copy(bf16[6144,256]{1,0:T(8,128)(2,1)} %all-gather.7.cloned.1.call-done) | data formatting | bytes 6291456 | tf_op jit(solution)/shard_map/while | solution.py:127
  137.3 56.1 %all-gather.9.cloned.1.call-done = bf16[6144,256]{1,0:T(8,128)(2,1)} async-done(((bf16[768,256]{1,0:T(8,128)(2,1)}), bf16[6144,256]{1,0:T(8,128)(2,1)}) %all-gather.9.cloned.1.call-update) | async-done | bytes 3145744 | tf_op jit(solution)/shard_map/all_gather | solution.py:190
  193.4 4.7 %copy.19 = bf16[6144,256]{0,1:T(8,128)(2,1)} copy(bf16[6144,256]{1,0:T(8,128)(2,1)} %all-gather.9.cloned.1.call-done) | data formatting | bytes 6291456 | tf_op jit(solution)/shard_map/while | solution.py:127
  198.2 67.8 %while.15 = (s32[]{:T(128)}, f32[768,4,64]{0,2,1:T(8,128)S(1)}, f32[4,768]{1,0:T(4,128)S(1)}, s32[768]{0:T(1024)S(1)}, bf16[6144,256]{0,1:T(8,128)(2,1)}, /*inde...) while((s32[]{:T(128)}, f32[768,4,64]{0,2,1:T(8,128)S(1)}, ...), condition=%wide.region_11.12_spmd, body=%wide.region_6.11_spmd.sunk | while | flops 775635520 | bytes 32112456 | solution.py:127
  199.4 7.2 %conditional.2 = ((f32[768,4,64]{0,2,1:T(8,128)S(1)}, f32[4,768]{1,0:T(4,128)S(1)})) conditional(s32[]{:T(128)} %convert_element_type.159, (f32[768,4,64]{0,2,1:T(8,128)S(1)}, f32[4,768]{1,0:T(4,128)S(1)}) %tuple.55, (s32[]{:T(128)}, bf16[6144,256]{0,1:T(8,128)(2,1)}, s32[768]{0:T(1024)S(1)}, bf16[6144,256]{0,1:T(8,128)(2,1)}, ...), branch_computations={%region_7.7_spmd, %region_8.10_spmd} | conditional | flops 775635520 | bytes 32112226 | solution.py:125
  201.9 2.6 fusion
  204.5 2.1 fusion.8
  207.9 7.2 %conditional.2 = ((f32[768,4,64]{0,2,1:T(8,128)S(1)}, f32[4,768]{1,0:T(4,128)S(1)})) conditional(s32[]{:T(128)} %convert_element_type.159, (f32[768,4,64]{0,2,1:T(8,128)S(1)}, f32[4,768]{1,0:T(4,128)S(1)}) %tuple.55, (s32[]{:T(128)}, bf16[6144,256]{0,1:T(8,128)(2,1)}, s32[768]{0:T(1024)S(1)}, bf16[6144,256]{0,1:T(8,128)(2,1)}, ...), branch_computations={%region_7.7_spmd, %region_8.10_spmd} | conditional | flops 775635520 | bytes 32112226 | solution.py:125
  210.3 2.6 fusion
  216.4 7.2 %conditional.2 = ((f32[768,4,64]{0,2,1:T(8,128)S(1)}, f32[4,768]{1,0:T(4,128)S(1)})) conditional(s32[]{:T(128)} %convert_element_type.159, (f32[768,4,64]{0,2,1:T(8,128)S(1)}, f32[4,768]{1,0:T(4,128)S(1)}) %tuple.55, (s32[]{:T(128)}, bf16[6144,256]{0,1:T(8,128)(2,1)}, s32[768]{0:T(1024)S(1)}, bf16[6144,256]{0,1:T(8,128)(2,1)}, ...), branch_computations={%region_7.7_spmd, %region_8.10_spmd} | conditional | flops 775635520 | bytes 32112226 | solution.py:125
  218.8 2.6 fusion
  224.8 7.2 %conditional.2 = ((f32[768,4,64]{0,2,1:T(8,128)S(1)}, f32[4,768]{1,0:T(4,128)S(1)})) conditional(s32[]{:T(128)} %convert_element_type.159, (f32[768,4,64]{0,2,1:T(8,128)S(1)}, f32[4,768]{1,0:T(4,128)S(1)}) %tuple.55, (s32[]{:T(128)}, bf16[6144,256]{0,1:T(8,128)(2,1)}, s32[768]{0:T(1024)S(1)}, bf16[6144,256]{0,1:T(8,128)(2,1)}, ...), branch_computations={%region_7.7_spmd, %region_8.10_spmd} | conditional | flops 775635520 | bytes 32112226 | solution.py:125
  227.3 2.6 fusion
  233.3 7.2 %conditional.2 = ((f32[768,4,64]{0,2,1:T(8,128)S(1)}, f32[4,768]{1,0:T(4,128)S(1)})) conditional(s32[]{:T(128)} %convert_element_type.159, (f32[768,4,64]{0,2,1:T(8,128)S(1)}, f32[4,768]{1,0:T(4,128)S(1)}) %tuple.55, (s32[]{:T(128)}, bf16[6144,256]{0,1:T(8,128)(2,1)}, s32[768]{0:T(1024)S(1)}, bf16[6144,256]{0,1:T(8,128)(2,1)}, ...), branch_computations={%region_7.7_spmd, %region_8.10_spmd} | conditional | flops 775635520 | bytes 32112226 | solution.py:125
  235.8 2.6 fusion
  241.8 7.2 %conditional.2 = ((f32[768,4,64]{0,2,1:T(8,128)S(1)}, f32[4,768]{1,0:T(4,128)S(1)})) conditional(s32[]{:T(128)} %convert_element_type.159, (f32[768,4,64]{0,2,1:T(8,128)S(1)}, f32[4,768]{1,0:T(4,128)S(1)}) %tuple.55, (s32[]{:T(128)}, bf16[6144,256]{0,1:T(8,128)(2,1)}, s32[768]{0:T(1024)S(1)}, bf16[6144,256]{0,1:T(8,128)(2,1)}, ...), branch_computations={%region_7.7_spmd, %region_8.10_spmd} | conditional | flops 775635520 | bytes 32112226 | solution.py:125
  244.2 2.6 fusion
  250.3 7.2 %conditional.2 = ((f32[768,4,64]{0,2,1:T(8,128)S(1)}, f32[4,768]{1,0:T(4,128)S(1)})) conditional(s32[]{:T(128)} %convert_element_type.159, (f32[768,4,64]{0,2,1:T(8,128)S(1)}, f32[4,768]{1,0:T(4,128)S(1)}) %tuple.55, (s32[]{:T(128)}, bf16[6144,256]{0,1:T(8,128)(2,1)}, s32[768]{0:T(1024)S(1)}, bf16[6144,256]{0,1:T(8,128)(2,1)}, ...), branch_computations={%region_7.7_spmd, %region_8.10_spmd} | conditional | flops 775635520 | bytes 32112226 | solution.py:125
  252.7 2.6 fusion
  258.7 7.2 %conditional.2 = ((f32[768,4,64]{0,2,1:T(8,128)S(1)}, f32[4,768]{1,0:T(4,128)S(1)})) conditional(s32[]{:T(128)} %convert_element_type.159, (f32[768,4,64]{0,2,1:T(8,128)S(1)}, f32[4,768]{1,0:T(4,128)S(1)}) %tuple.55, (s32[]{:T(128)}, bf16[6144,256]{0,1:T(8,128)(2,1)}, s32[768]{0:T(1024)S(1)}, bf16[6144,256]{0,1:T(8,128)(2,1)}, ...), branch_computations={%region_7.7_spmd, %region_8.10_spmd} | conditional | flops 775635520 | bytes 32112226 | solution.py:125
  261.2 2.6 fusion
  266.0 5.5 %add_convert_fusion.1 = bf16[768,2048]{1,0:T(8,128)(2,1)} fusion(f32[768,2048]{1,0:T(8,128)} %fusion.49, bf16[768,256]{0,1:T(8,128)(2,1)S(1)} %bitcast.48, bf16[256,2048]{1,0:T(8,128)(2,1)S(1)} %copy-done.4), kind=kOutput, calls=%fused_computation.39 | convolution fusion | flops 808452096 | bytes 10878976 | tf_op jit(solution)/shard_map/dot_general | solution.py:202
  271.6 38.0 %reduce-scatter.2.cloned.1.call-done = bf16[192,2048]{1,0:T(8,128)(2,1)} async-done(((bf16[768,2048]{1,0:T(8,128)(2,1)}), bf16[192,2048]{1,0:T(8,128)(2,1)}) %reduce-scatter.2.cloned.1.call-update) | async-done | bytes 786448 | tf_op jit(solution)/shard_map/reduce_scatter | solution.py:201
  (216 shorter events, 53.3 us)
Async XLA Ops:
  6.5 96.4 %copy-start = (bf16[256,2048]{1,0:T(8,128)(2,1)S(1)}, bf16[256,2048]{1,0:T(8,128)(2,1)}, u32[]{:S(2)}) copy-start(bf16[256,2048]{1,0:T(8,128)(2,1)} %param.34) | copy-start | bytes 3145732
  6.5 33.6 %copy-start.9 = (f32[2048]{0:T(1024)S(1)}, f32[2048]{0:T(1024)}, u32[]{:S(2)}) copy-start(f32[2048]{0:T(1024)} %param.21) | copy-start | bytes 24580
  6.5 30.9 %all-gather.5.cloned.1.call-start = ((), (), s32[]{:S(2)}) async-start(), calls=%async_computation.1 | async-start | bytes 3932160 | tf_op jit(solution)/shard_map/all_gather | solution.py:148
  7.3 100.9 %all-gather.11.cloned.1.call-start = ((), (), s32[]{:S(2)}) async-start(), calls=%async_computation.4 | async-start | bytes 1474560 | tf_op jit(solution)/shard_map/all_gather | solution.py:173
  37.4 2.8 copy-start.3
  40.3 1.0 copy-start.6
  41.3 2.9 copy-start.1
  41.3 1.7 copy-start.12
  43.0 17.8 %copy-start.14 = (bf16[512,256]{1,0:T(8,128)(2,1)S(1)}, bf16[512,256]{1,0:T(8,128)(2,1)}, u32[]{:S(2)}) copy-start(bf16[512,256]{1,0:T(8,128)(2,1)} %param.31) | copy-start | bytes 786436
  52.1 12.6 %copy-start.11 = (bf16[2048,256]{1,0:T(8,128)(2,1)S(1)}, bf16[2048,256]{1,0:T(8,128)(2,1)}, u32[]{:S(2)}) copy-start(bf16[2048,256]{1,0:T(8,128)(2,1)} %param.22) | copy-start | bytes 3145732
  52.1 80.5 %all-gather.7.cloned.1.call-start = ((), (), s32[]{:S(2)}) async-start(), calls=%async_computation.2 | async-start | bytes 3538944 | tf_op jit(solution)/shard_map/all_gather | solution.py:191
  62.0 131.4 %all-gather.9.cloned.1.call-start = ((), (), s32[]{:S(2)}) async-start(), calls=%async_computation.3 | async-start | bytes 3538944 | tf_op jit(solution)/shard_map/all_gather | solution.py:190
  64.2 245.4 %reduce-scatter.2.cloned.1.call-start = ((), (), s32[]{:S(2)}) async-start(), calls=%async_computation.5 | async-start | bytes 3932160 | tf_op jit(solution)/shard_map/reduce_scatter | solution.py:201
  64.7 4.4 %copy-start.2 = (bf16[768,2048]{1,0:T(8,128)(2,1)S(1)}, bf16[768,2048]{1,0:T(8,128)(2,1)}, u32[]{:S(2)}) copy-start(bf16[768,2048]{1,0:T(8,128)(2,1)} %copy-done.1) | copy-start | bytes 9437188
  64.7 4.4 %copy-start.7 = (bf16[2048,32]{0,1:T(8,128)(2,1)S(1)}, bf16[2048,32]{0,1:T(8,128)(2,1)}, u32[]{:S(2)}) copy-start(bf16[2048,32]{0,1:T(8,128)(2,1)} %param.26) | copy-start | bytes 393220
  67.8 35.1 %copy-start.15 = (f32[256]{0:T(256)S(1)}, f32[256]{0:T(256)}, u32[]{:S(2)}) copy-start(f32[256]{0:T(256)} %param.23) | copy-start | bytes 3076
  67.8 35.0 %collective-permute-start = (bf16[15,256]{1,0:T(8,128)(2,1)S(1)}, bf16[15,256]{1,0:T(8,128)(2,1)S(1)}, u32[]{:S(2)}, u32[]{:S(2)}) collective-permute-start(bf16[15,256]{1,0:T(8,128)(2,1)S(1)} %slice.102), channel_id=1, source_target_pairs={{0,4},{4,8},{8,12},{12,16},{16,20},{20,24},{24,28},{1,5},{5,9},{9,... | collective-permute-start | bytes 23048 | tf_op jit(solution)/shard_map/ppermute | solution.py:25
  102.9 5.2 %copy-start.13 = (bf16[768,384]{1,0:T(8,128)(2,1)S(1)}, bf16[768,384]{1,0:T(8,128)(2,1)}, u32[]{:S(2)}) copy-start(bf16[768,384]{1,0:T(8,128)(2,1)} %param.29) | copy-start | bytes 1769476
  108.2 2.2 copy-start.10
  137.3 60.9 %copy-start.8 = (f32[96]{0:T(128)S(1)}, f32[96]{0:T(128)}, u32[]{:S(2)}) copy-start(f32[96]{0:T(128)} %param.33) | copy-start | bytes 1156
  198.1 67.9 %copy-start.4 = (bf16[256,2048]{1,0:T(8,128)(2,1)S(1)}, bf16[256,2048]{1,0:T(8,128)(2,1)}, u32[]{:S(2)}) copy-start(bf16[256,2048]{1,0:T(8,128)(2,1)} %param.35) | copy-start | bytes 3145732
  199.5 2.4 copy-start.5
  207.9 2.4 copy-start.5
  216.4 2.4 copy-start.5
  224.9 2.4 copy-start.5
  233.4 2.4 copy-start.5
  241.8 2.4 copy-start.5
  250.3 2.4 copy-start.5
  258.8 2.4 copy-start.5
Sparse Core Ops, SparseCore 0:
  8.9 28.4 all-gather.4
  52.3 17.4 all-gather.10
  72.0 60.6 all-gather.6
  134.7 58.6 all-gather.8
  271.7 37.8 reduce-scatter.1
where the time goes:
time: 320 us; the launch traced here: 316 us
  waiting for transfers between devices  145 us (45%)
  matrix products  60.3 us (19%)
  blocking collectives  47.4 us (15%)
  local copies, waits for them, and re-layouts  27.3 us (9%)
  other arithmetic  14.6 us (5%)
  between operations  13.5 us (4%)
  loops' own time  6.11 us (2%)
    all_gather x1, waiting for transfers between devices, local(): lax.all_gather(key_plain, 'sp', axis=0, tiled=True)  56.1 us
    reduce_scatter x1, waiting for transfers between devices, local(): lax.psum_scatter((term + jnp.dot(attended, w_out_attn, preferred_element_...  38 us
    all_gather x1, blocking collectives, local(): lax.all_gather(rope_key, 'sp', axis=0, tiled=True)  32.6 us
    all_gather x1, waiting for transfers between devices, local(): own_input = lax.all_gather(activations, 'tp', axis=0, tiled=True)  29.4 us
    all_gather x1, waiting for transfers between devices, local(): lax.all_gather(value_rows, 'sp', axis=0, tiled=True)  21.2 us
    dot_general x8, matrix products, update(): jnp.einsum('qhd,khd->hqk', queries, key_rows, preferred_element_type=jnp....  21.1 us
    dot_general x8, matrix products, update(): jnp.einsum('hqk,khd->qhd', weights.astype(jnp.bfloat16), value_rows, pref...  16.7 us
    dynamic_slice x16, local copies, waits for them, and re-layouts, accumulate(): lax.dynamic_slice_in_dim(member, offset, block_size, 0)  9.99 us
  transfers between devices with their start and end apart: 6, of which 4 were waited for; matrix products, arithmetic and copies ran while one was open for 7% of the time, Pallas kernels for 0%

commit v1 on v0

v1 whole, which is shorter than its diff:
```python
import functools
import math

import jax
import jax.numpy as jnp
from jax import lax
from jax.experimental import pallas as pl
from jax.experimental.pallas import tpu as pltpu
from jax.sharding import PartitionSpec as P

GROUP = 256
NOPE = 64
ROPE = 32
VDIM = 64
HEAD = NOPE + ROPE
LANES = 128

norm_eps = 1e-06
rope_theta = 10000.0
rim_depth = 15
bf16 = jnp.bfloat16
f32 = jnp.float32


def from_behind(block, axis, distance):
    devices = range(lax.axis_size(axis))
    route = [(i - distance, i) for i in devices if i - distance in devices]
    return lax.ppermute(block, axis, route)


def row_norm(source, norm_gain):
    as_float = source.astype(f32)
    factor = lax.rsqrt(jnp.mean(as_float * as_float, axis=-1, keepdims=True) + norm_eps)
    return as_float * factor * norm_gain


def pool_mix(extended, positions, channel_start):
    row_count = positions.shape[0]
    width = extended.shape[1]
    channel = channel_start + jnp.arange(width, dtype=jnp.int32)
    window = jnp.left_shift(jnp.int32(2), channel // GROUP)
    as_float = extended.astype(f32)
    total = as_float
    window_sum = None
    for level in range(4):
        span = 1 << level
        total = total + jnp.concatenate([jnp.zeros((span, width), f32), total[:-span]], axis=0)
        chosen = total[rim_depth:]
        if window_sum is None:
            window_sum = chosen
        else:
            window_sum = jnp.where(window[None, :] >= 2 * span, chosen, window_sum)
    divisor = jnp.minimum(positions[:, None] + 1, window[None, :]).astype(f32)
    return window_sum / divisor - as_float[rim_depth:]


def pad_heads(weight, width):
    depth = weight.shape[0]
    heads = weight.shape[1] // width
    shaped = weight.reshape(depth, heads, width)
    return jnp.pad(shaped, ((0, 0), (0, 0), (0, LANES - width))).reshape(depth, heads * LANES)


def pad_row(gain):
    return jnp.pad(gain, (0, LANES - gain.shape[0])).reshape(1, LANES)


def rope_tables(rows, blocks):
    half = ROPE // 2
    frequency = rope_theta ** (-jnp.arange(0, ROPE, 2, dtype=f32) / ROPE)

    def make(positions):
        angles = positions.astype(f32)[:, None] * frequency[None, :]
        cosine, sine = jnp.cos(angles), jnp.sin(angles)
        count = positions.shape[0]
        rest = LANES - HEAD
        cos_row = jnp.concatenate(
            [jnp.ones((count, NOPE), f32), cosine, cosine, jnp.zeros((count, rest), f32)], axis=1
        )
        sin_row = jnp.concatenate(
            [jnp.zeros((count, NOPE), f32), sine, sine, jnp.zeros((count, rest), f32)], axis=1
        )
        return cos_row, sin_row

    return make(jnp.arange(rows)) + make(jnp.arange(blocks) * rows)


def head_finish(x, gain, cosine, sin_low, sin_high):
    factor = lax.rsqrt(jnp.sum(x * x, axis=1, keepdims=True) * (1.0 / HEAD) + norm_eps)
    y = x * factor * gain
    half = ROPE // 2
    return (
        y * cosine
        + pltpu.roll(y, LANES - half, 1) * sin_low
        + pltpu.roll(y, half, 1) * sin_high
    )


def attention_kernel(
    heads,
    step_rows,
    q_ref,
    kv_ref,
    wq_ref,
    wk_ref,
    wv_ref,
    qlat_gain,
    kvlat_gain,
    qh_gain,
    kh_gain,
    cos_r,
    sin_r,
    cos_b,
    sin_b,
    out_ref,
    kv_buf,
    queries,
    keys_t,
    values,
    acc,
    sem,
):
    rows = q_ref.shape[0]
    kvlat = wk_ref.shape[0]
    mine = lax.axis_index("sp")
    lane = lax.broadcasted_iota(jnp.int32, (step_rows, LANES), 1)
    score_scale = HEAD ** (-0.5) * math.log2(math.e)

    def fetch(block, slot):
        return pltpu.make_async_copy(kv_ref.at[block], kv_buf.at[slot], sem.at[slot])

    fetch(0, 0).start()

    def angles(block, at):
        cr, sr = cos_r[at, :], sin_r[at, :]
        cb, sb = cos_b[pl.ds(block, 1), :], sin_b[pl.ds(block, 1), :]
        cosine = jnp.where(lane < NOPE, 1.0, cr * cb - sr * sb)
        sine = sr * cb + cr * sb
        low = jnp.where((lane >= NOPE) & (lane < NOPE + ROPE // 2), -sine, 0.0)
        high = jnp.where((lane >= NOPE + ROPE // 2) & (lane < HEAD), sine, 0.0)
        return cosine, low, high

    def prepare_queries(step, _):
        at = pl.ds(pl.multiple_of(step * step_rows, step_rows), step_rows)
        normed = row_norm(q_ref[at, :], qlat_gain[...]).astype(bf16)
        raw = jnp.dot(normed, wq_ref[...], preferred_element_type=f32).astype(bf16).astype(f32)
        tables = angles(mine, at)
        for h in range(heads):
            x = raw[:, h * LANES : (h + 1) * LANES]
            y = head_finish(x, qh_gain[...], *tables)
            queries[h, at, :] = (y * score_scale).astype(bf16)
        return 0

    lax.fori_loop(0, rows // step_rows, prepare_queries, 0)
    acc[...] = jnp.zeros_like(acc)

    def prepare_keys(block, slot):
        def one(step, _):
            at = pl.ds(pl.multiple_of(step * step_rows, step_rows), step_rows)
            latent = kv_buf[slot, at, :kvlat]
            shared = kv_buf[slot, at, kvlat:].astype(f32)
            normed = row_norm(latent, kvlat_gain[...]).astype(bf16)
            plain = jnp.dot(normed, wk_ref[...], preferred_element_type=f32).astype(bf16).astype(f32)
            value = jnp.dot(normed, wv_ref[...], preferred_element_type=f32)
            tables = angles(block, at)
            for h in range(heads):
                x = plain[:, h * LANES : (h + 1) * LANES] + shared
                y = head_finish(x, kh_gain[...], *tables)
                keys_t[h, :, at] = y.T.astype(bf16)
                v = jnp.where(lane == VDIM, 1.0, value[:, h * LANES : (h + 1) * LANES])
                values[h, at, :] = v.astype(bf16)
            return 0

        lax.fori_loop(0, rows // step_rows, one, 0)

    def accumulate(on_diagonal):
        def one(step, _):
            at = pl.ds(pl.multiple_of(step * step_rows, step_rows), step_rows)
            for h in range(heads):
                scores = jnp.dot(queries[h, at, :], keys_t[h], preferred_element_type=f32)
                weights = jnp.exp2(scores)
                if on_diagonal:
                    q_pos = step * step_rows + lax.broadcasted_iota(jnp.int32, scores.shape, 0)
                    k_pos = lax.broadcasted_iota(jnp.int32, scores.shape, 1)
                    weights = jnp.where(k_pos <= q_pos, weights, 0.0)
                acc[h, at, :] += jnp.dot(weights.astype(bf16), values[h], preferred_element_type=f32)
            return 0

        lax.fori_loop(0, rows // step_rows, one, 0)

    def earlier(block, _):
        slot = lax.rem(block, 2)
        fetch(block, slot).wait()
        fetch(block + 1, 1 - slot).start()
        prepare_keys(block, slot)
        accumulate(False)
        return 0

    lax.fori_loop(0, mine, earlier, 0)
    slot = lax.rem(mine, 2)
    fetch(mine, slot).wait()
    prepare_keys(mine, slot)
    accumulate(True)

    def finish(step, _):
        at = pl.ds(pl.multiple_of(step * step_rows, step_rows), step_rows)
        parts = []
        for h in range(heads):
            a = acc[h, at, :]
            parts.append(a[:, :VDIM] / a[:, VDIM : VDIM + 1])
        out_ref[at, :] = jnp.concatenate(parts, axis=1).astype(bf16)
        return 0

    lax.fori_loop(0, rows // step_rows, finish, 0)


def attention(q_lat, kv_all, wq, wk, wv, gains, tables):
    rows = q_lat.shape[0]
    heads = wq.shape[1] // LANES
    step_rows = math.gcd(rows, 256)
    vm = pl.BlockSpec(memory_space=pltpu.VMEM)
    return pl.pallas_call(
        functools.partial(attention_kernel, heads, step_rows),
        out_shape=jax.ShapeDtypeStruct((rows, heads * VDIM), bf16),
        in_specs=[vm, pl.BlockSpec(memory_space=pl.ANY)] + [vm] * 11,
        out_specs=vm,
        scratch_shapes=[
            pltpu.VMEM((2,) + kv_all.shape[1:], bf16),
            pltpu.VMEM((heads, rows, LANES), bf16),
            pltpu.VMEM((heads, LANES, rows), bf16),
            pltpu.VMEM((heads, rows, LANES), bf16),
            pltpu.VMEM((heads, rows, LANES), f32),
            pltpu.SemaphoreType.DMA((2,)),
        ],
        compiler_params=pltpu.CompilerParams(vmem_limit_bytes=48 * 1024 * 1024),
    )(q_lat, kv_all, wq, wk, wv, *gains, *tables)


def local(
    activations,
    in_gain,
    w_pool_in,
    pool_gain,
    w_qlat,
    w_kvlat,
    w_krope,
    qlat_gain,
    kvlat_gain,
    w_qup,
    w_kup,
    w_vup,
    qhead_gain,
    khead_gain,
    w_out_pool,
    w_out_attn,
):
    own_input = lax.all_gather(activations, "tp", axis=0, tiled=True)
    row_count = own_input.shape[0]
    n_sp = lax.axis_size("sp")
    positions = lax.axis_index("sp") * row_count + jnp.arange(row_count, dtype=jnp.int32)
    normed = row_norm(own_input, in_gain).astype(bf16)
    q_part = jnp.dot(normed, w_qlat, preferred_element_type=f32).astype(bf16)
    kv_part = jnp.dot(normed, w_kvlat, preferred_element_type=f32).astype(bf16)
    krope_pad = jnp.pad(w_krope, ((0, 0), (NOPE, LANES - HEAD)))
    rope_key = jnp.dot(normed, krope_pad, preferred_element_type=f32).astype(bf16)
    q_width = q_part.shape[1]
    latents = lax.all_gather(jnp.concatenate([q_part, kv_part], axis=1), "tp", axis=0, tiled=False)
    q_lat = jnp.concatenate([latents[i, :, :q_width] for i in range(latents.shape[0])], axis=1)
    kv_lat = jnp.concatenate(
        [latents[i, :, q_width:] for i in range(latents.shape[0])] + [rope_key], axis=1
    )
    kv_all = lax.all_gather(kv_lat, "sp", axis=0, tiled=False)
    pool_in = jnp.dot(normed, w_pool_in, preferred_element_type=f32).astype(bf16)
    prev_rows = from_behind(pool_in[row_count - rim_depth :], "sp", 1)
    extended = jnp.concatenate([prev_rows, pool_in], axis=0)
    channel_start = lax.axis_index("tp") * pool_in.shape[1]
    pool_out = (pool_mix(extended, positions, channel_start) * pool_gain).astype(bf16)
    attended = attention(
        q_lat,
        kv_all,
        pad_heads(w_qup, HEAD),
        pad_heads(w_kup, NOPE),
        pad_heads(w_vup, VDIM),
        (qlat_gain.reshape(1, -1), kvlat_gain.reshape(1, -1), pad_row(qhead_gain), pad_row(khead_gain)),
        rope_tables(row_count, n_sp),
    )
    term = jnp.dot(pool_out, w_out_pool, preferred_element_type=f32)
    return lax.psum_scatter(
        (term + jnp.dot(attended, w_out_attn, preferred_element_type=f32)).astype(bf16),
        "tp",
        scatter_dimension=0,
        tiled=True,
    )


def solution(mesh):
    placed = (
        P(("sp", "tp"), None),
        P(),
        P(None, "tp"),
        P("tp"),
        P(None, "tp"),
        P(None, "tp"),
        P(),
        P(),
        P(),
        P(None, "tp"),
        P(None, "tp"),
        P(None, "tp"),
        P(),
        P(),
        P("tp", None),
        P("tp", None),
    )
    return jax.shard_map(
        local, mesh=mesh, in_specs=placed, out_specs=P(("sp", "tp"), None), check_vma=False
    )
```

time: 320 us -> 305 us (0.953)
  Pallas kernels: 0 us -> 56.7 us
  blocking collectives: 47.4 us -> 0 us
  matrix products: 60.3 us -> 16 us
  waiting for transfers between devices: 145 us -> 185 us
  local copies, waits for them, and re-layouts: 27.3 us -> 16.4 us
  loops' own time: 6.11 us -> 0 us
    pallas_call x0 -> x1, Pallas kernels: none -> 56.7 us  [attention(): pl.pallas_call(functools.partial(attention_kernel, heads, step_rows), out...]
    dot_general x25 -> x6, matrix products: 60.3 us -> 16 us  [the longest x1 4.07 us: local(): term = jnp.dot(pool_out, w_out_pool, preferred_element_type=f32)]
    all_gather x2 -> x0, blocking collectives: 40.3 us -> none  [the longest x1 32.6 us: local(): lax.all_gather(rope_key, 'sp', axis=0, tiled=True)]
    all_gather x3 -> x2, waiting for transfers between devices: 77.3 us -> 116 us  [the longest x1 93.6 us: local(): kv_all = lax.all_gather(kv_lat, 'sp', axis=0, tiled=False)]
    dynamic_slice x18 -> x0, local copies, waits for them, and re-layouts: 11.6 us -> none  [the longest x16 9.99 us: accumulate(): lax.dynamic_slice_in_dim(member, offset, block_size, 0)]
    unnamed x30 -> x61, local copies, waits for them, and re-layouts: 0.88 us -> 10.4 us
    while x2 -> x0, local copies, waits for them, and re-layouts: 9.32 us -> none  [sweep(): return lax.fori_loop(0, piece_rows // block_size, advance, state_pair)]
    psum x1 -> x0, blocking collectives: 7.07 us -> none  [local(): lax.psum((jnp.sum(q_float * q_float, axis=1), jnp.sum(kv_float * kv_float...]
  transfers between devices with their start and end apart: 6 -> 5, of which waited for: 4 -> 5; matrix products, arithmetic and copies ran while one was open for 7% -> 6% of each run, Pallas kernels for 0% -> 0%
where the time goes in v1:
time: 305 us; the launch traced here: 302 us
  waiting for transfers between devices  185 us (61%)
  Pallas kernels  56.7 us (19%)
  local copies, waits for them, and re-layouts  16.4 us (5%)
  matrix products  16 us (5%)
  between operations  13.5 us (4%)
  other arithmetic  12.1 us (4%)
    all_gather x1, waiting for transfers between devices, local(): kv_all = lax.all_gather(kv_lat, 'sp', axis=0, tiled=False)  93.6 us
    pallas_call x1, Pallas kernels, attention(): pl.pallas_call(functools.partial(attention_kernel, heads, step_rows), out...  56.7 us
    reduce_scatter x1, waiting for transfers between devices, local(): lax.psum_scatter((term + jnp.dot(attended, w_out_attn, preferred_element_...  38 us
    all_gather x1, waiting for transfers between devices, local(): own_input = lax.all_gather(activations, 'tp', axis=0, tiled=True)  30.1 us
    all_gather x1, waiting for transfers between devices, local(): lax.all_gather(jnp.concatenate([q_part, kv_part], axis=1), 'tp', axis=0,...  21.9 us
    unnamed x61, local copies, waits for them, and re-layouts  10.4 us
  transfers between devices with their start and end apart: 5, of which 5 were waited for; matrix products, arithmetic and copies ran while one was open for 6% of the time, Pallas kernels for 0%

profile of v1, /device:TPU:30, one launch (start us, length us, event | category | flops | bytes accessed | tf_op | source)
XLA Modules:
  0.0 301.6 jit_solution(17675952947780261375)
XLA Ops:
  6.5 0.7 all-gather.6.cloned.1.call-update
  7.3 30.1 %all-gather.6.cloned.1.call-done = bf16[768,2048]{1,0:T(8,128)(2,1)} async-done(((bf16[192,2048]{1,0:T(8,128)(2,1)}), bf16[768,2048]{1,0:T(8,128)(2,1)}) %all-gather.6.cloned.1.call-update) | async-done | bytes 3145744 | tf_op jit(solution)/shard_map/all_gather | solution.py:257
  37.4 2.7 fusion
  40.3 0.8 fusion.2
  41.4 1.2 convolution_convert_fusion.1
  42.8 1.2 convolution_convert_fusion.3
  44.0 0.8 pad_maximum_fusion.1
  44.9 21.9 %all-gather.8.cloned.1.call-done = bf16[3072,320]{0,1:T(8,128)(2,1)} async-done(((bf16[768,320]{0,1:T(8,128)(2,1)}), bf16[3072,320]{0,1:T(8,128)(2,1)}) %all-gather.8.cloned.1.call-update) | async-done | bytes 1966096 | tf_op jit(solution)/shard_map/all_gather | solution.py:267
  66.8 2.9 copy.27
  69.8 1.0 fusion.21
  70.7 0.8 fusion.20
  71.6 0.9 fusion.19
  72.4 0.9 fusion.18
  73.3 3.6 %fusion.3 = bf16[768,640]{1,0:T(8,128)(2,1)} fusion(bf16[768,640]{1,0:T(8,128)(2,1)} %fusion.18, bf16[768,2048]{1,0:T(8,128)(2,1)} %copy-done.7, bf16[2048,32]{0,1:T(8,128)(2,1)S(1)} %copy-done.21), kind=kOutput, calls=%fused_computation.10 | convolution fusion | flops 402751488 | bytes 3473408 | tf_op jit(solution)/shard_map/dot_general | solution.py:265
  79.7 1.4 multiply_sine_fusion
  81.1 1.4 maximum_maximum_fusion.1
  82.5 3.2 %convolution_convert_fusion = bf16[768,256]{1,0:T(8,128)(2,1)S(1)} fusion(bf16[768,2048]{1,0:T(8,128)(2,1)} %copy-done.7, bf16[2048,256]{1,0:T(8,128)(2,1)} %param.18), kind=kOutput, calls=%fused_computation.6 | convolution fusion | flops 805502976 | bytes 4587520 | tf_op jit(solution)/shard_map/dot_general | solution.py:273
  86.4 1.5 collective-permute-start
  89.4 1.1 copy.33
  90.6 1.0 copy.39.wv_ref
  91.6 0.9 collective-permute-done
  92.5 0.8 maximum_convert_fusion
  93.3 0.9 pad_add_fusion.2
  94.9 4.1 %fusion.10 = f32[768,2048]{1,0:T(8,128)} fusion(bf16[256,2048]{1,0:T(8,128)(2,1)S(1)} %copy-done, f32[783,256]{1,0:T(8,128)S(1)} %maximum_convert_fusion, f32[783,256]{1,0:T(8,128)S(1)} %pad_add_fusion.2, f32[783,256]{1,0:T(8,128)S(1)} %pad_add_fusion.1, f32[775,256]{1,0:T(8,128)S(1)} %slice.76, f32[783,256]{1,0:T(8,128)S(1)} %pad_add_fusion, ...), kind=kOutput, calls=%fused_computation.28 | convolution fusion | flops 807272448 | bytes 11288064 | tf_op jit(solution)/shard_map/dot_general | solution.py:287
  99.6 93.6 %all-gather.10.cloned.1.call-done = bf16[6144,640]{1,0:T(8,128)(2,1)} async-done(((bf16[768,640]{1,0:T(8,128)(2,1)}), bf16[6144,640]{1,0:T(8,128)(2,1)}) %all-gather.10.cloned.1.call-update) | async-done | bytes 7864336 | tf_op jit(solution)/shard_map/all_gather | solution.py:272
  193.2 1.0 copy-done.1
  194.3 1.0 copy-done.2
  195.2 1.0 copy-done.3
  196.9 0.7 copy-done.5
  197.6 56.7 %shard_map.154 = bf16[768,256]{1,0:T(8,128)(2,1)S(1)} custom-call(bf16[768,768]{1,0:T(8,128)(2,1)S(1)} %pad_maximum_fusion.q_ref, bf16[8,768,640]{2,1,0:T(8,128)(2,1)} %bitcast.56, bf16[768,512]{1,0:T(8,128)(2,1)S(1)} %copy.37.wq_ref, bf16[512,512]{1,0:T(8,128)(2,1)S(1)} %copy.38.wk_ref, bf16[512,512]{1,0:T(8,128)(2,1)S(1)} %copy-done.1, ...), custom_call_target="tpu_custom_call" | custom-call | tf_op jit(solution)/shard_map/pallas_call | solution.py:222
  254.3 2.7 add_convert_fusion
  257.0 38.0 %reduce-scatter.2.cloned.1.call-done = bf16[192,2048]{1,0:T(8,128)(2,1)} async-done(((bf16[768,2048]{1,0:T(8,128)(2,1)}), bf16[192,2048]{1,0:T(8,128)(2,1)}) %reduce-scatter.2.cloned.1.call-update) | async-done | bytes 786448 | tf_op jit(solution)/shard_map/reduce_scatter | solution.py:288
  (88 shorter events, 7.6 us)
Async XLA Ops:
  6.5 88.0 %copy-start = (bf16[256,2048]{1,0:T(8,128)(2,1)S(1)}, bf16[256,2048]{1,0:T(8,128)(2,1)}, u32[]{:S(2)}) copy-start(bf16[256,2048]{1,0:T(8,128)(2,1)} %param.30) | copy-start | bytes 3145732
  6.5 33.6 %copy-start.15 = (f32[2048]{0:T(1024)S(1)}, f32[2048]{0:T(1024)}, u32[]{:S(2)}) copy-start(f32[2048]{0:T(1024)} %param.17) | copy-start | bytes 24580
  6.5 30.9 %all-gather.6.cloned.1.call-start = ((), (), s32[]{:S(2)}) async-start(), calls=%async_computation.1 | async-start | bytes 3932160 | tf_op jit(solution)/shard_map/all_gather | solution.py:257
  7.3 59.6 %all-gather.8.cloned.1.call-start = ((), (), s32[]{:S(2)}) async-start(), calls=%async_computation.3 | async-start | bytes 2457600 | tf_op jit(solution)/shard_map/all_gather | solution.py:267
  37.4 2.8 copy-start.6
  40.3 1.1 copy-start.20
  41.4 2.6 copy-start.7
  41.4 1.4 copy-start.13
  44.8 28.5 %copy-start.21 = (bf16[2048,32]{0,1:T(8,128)(2,1)S(1)}, bf16[2048,32]{0,1:T(8,128)(2,1)}, u32[]{:S(2)}) copy-start(bf16[2048,32]{0,1:T(8,128)(2,1)} %param.22) | copy-start | bytes 393220
  44.8 148.4 %all-gather.10.cloned.1.call-start = ((), (), s32[]{:S(2)}) async-start(), calls=%async_computation.4 | async-start | bytes 8847360 | tf_op jit(solution)/shard_map/all_gather | solution.py:272
  69.7 7.2 %copy-start.8 = (bf16[3072,320]{1,0:T(8,128)(2,1)}, bf16[3072,320]{1,0:T(8,128)(2,1)S(1)}, u32[]{:S(2)}) copy-start(bf16[3072,320]{1,0:T(8,128)(2,1)S(1)} %copy.27) | copy-start | bytes 5898244
  73.3 5.0 %copy-start.18 = (f32[96]{0:T(128)S(1)}, f32[96]{0:T(128)}, u32[]{:S(2)}) copy-start(f32[96]{0:T(128)} %param.29) | copy-start | bytes 1156
  73.3 5.0 %copy-start.19 = (f32[96]{0:T(128)S(1)}, f32[96]{0:T(128)}, u32[]{:S(2)}) copy-start(f32[96]{0:T(128)} %param.28) | copy-start | bytes 1156
  76.9 218.1 %reduce-scatter.2.cloned.1.call-start = ((), (), s32[]{:S(2)}) async-start(), calls=%async_computation.2 | async-start | bytes 3932160 | tf_op jit(solution)/shard_map/reduce_scatter | solution.py:288
  82.5 5.9 %copy-start.12 = (bf16[768,384]{1,0:T(8,128)(2,1)S(1)}, bf16[768,384]{1,0:T(8,128)(2,1)}, u32[]{:S(2)}) copy-start(bf16[768,384]{1,0:T(8,128)(2,1)} %param.25) | copy-start | bytes 1769476
  85.7 3.3 %copy-start.14 = (bf16[512,256]{1,0:T(8,128)(2,1)S(1)}, bf16[512,256]{1,0:T(8,128)(2,1)}, u32[]{:S(2)}) copy-start(bf16[512,256]{1,0:T(8,128)(2,1)} %param.26) | copy-start | bytes 786436
  86.4 6.1 %collective-permute-start = (bf16[15,256]{1,0:T(8,128)(2,1)}, bf16[15,256]{1,0:T(8,128)(2,1)}, u32[]{:S(2)}, u32[]{:S(2)}) collective-permute-start(bf16[15,256]{1,0:T(8,128)(2,1)} %slice.72), channel_id=1, source_target_pairs={{0,4},{4,8},{8,12},{12,16},{16,20},{20,24},{24,28},{1,5},{5,9},{9,... | collective-permute-start | bytes 23048 | tf_op jit(solution)/shard_map/ppermute | solution.py:28
  88.7 2.9 copy-start.16
  94.1 0.7 copy-start.17
  94.2 0.7 copy-start.22
  94.2 0.7 copy-start.23
  94.2 0.7 copy-start.24
  94.2 0.7 copy-start.25
  94.2 0.7 copy-start.26
  94.9 4.1 %copy-start.9 = (bf16[3072,320]{1,0:T(8,128)(2,1)S(1)}, bf16[3072,320]{1,0:T(8,128)(2,1)}, u32[]{:S(2)}) copy-start(bf16[3072,320]{1,0:T(8,128)(2,1)} %copy-done.8) | copy-start | bytes 5898244
  193.2 1.0 copy-start.1
  194.3 1.0 copy-start.2
  195.2 1.0 copy-start.3
  196.2 0.7 copy-start.4
  196.9 0.7 copy-start.5
  197.6 56.7 %copy-start.10 = (f32[768,2048]{1,0:T(8,128)S(1)}, f32[768,2048]{1,0:T(8,128)}, u32[]{:S(2)}) copy-start(f32[768,2048]{1,0:T(8,128)} %fusion.10) | copy-start | bytes 18874372
  197.6 56.7 %copy-start.11 = (bf16[256,2048]{1,0:T(8,128)(2,1)S(1)}, bf16[256,2048]{1,0:T(8,128)(2,1)}, u32[]{:S(2)}) copy-start(bf16[256,2048]{1,0:T(8,128)(2,1)} %param.31) | copy-start | bytes 3145732
Sparse Core Ops, SparseCore 0:
  8.9 28.4 all-gather.5
  45.0 21.8 all-gather.7
  77.0 116.1 all-gather.9
  257.1 37.8 reduce-scatter.1

commit v2 on v1

--- a/solution.py
+++ b/solution.py
@@ -101,6 +101,7 @@
     step_rows,
     q_ref,
     kv_ref,
+    own_ref,
     wq_ref,
     wk_ref,
     wv_ref,
@@ -118,7 +119,9 @@
     keys_t,
     values,
     acc,
+    own_buf,
     sem,
+    own_sem,
 ):
     rows = q_ref.shape[0]
     kvlat = wk_ref.shape[0]
@@ -129,7 +132,12 @@
     def fetch(block, slot):
         return pltpu.make_async_copy(kv_ref.at[block], kv_buf.at[slot], sem.at[slot])
 
-    fetch(0, 0).start()
+    own_copy = pltpu.make_async_copy(own_ref, own_buf, own_sem)
+    own_copy.start()
+
+    @pl.when(mine > 0)
+    def _():
+        fetch(0, 0).start()
 
     def angles(block, at):
         cr, sr = cos_r[at, :], sin_r[at, :]
@@ -154,11 +162,11 @@
     lax.fori_loop(0, rows // step_rows, prepare_queries, 0)
     acc[...] = jnp.zeros_like(acc)
 
-    def prepare_keys(block, slot):
+    def prepare_keys(block, source):
         def one(step, _):
             at = pl.ds(pl.multiple_of(step * step_rows, step_rows), step_rows)
-            latent = kv_buf[slot, at, :kvlat]
-            shared = kv_buf[slot, at, kvlat:].astype(f32)
+            latent = source[at, :kvlat]
+            shared = source[at, kvlat:].astype(f32)
             normed = row_norm(latent, kvlat_gain[...]).astype(bf16)
             plain = jnp.dot(normed, wk_ref[...], preferred_element_type=f32).astype(bf16).astype(f32)
             value = jnp.dot(normed, wv_ref[...], preferred_element_type=f32)
@@ -191,15 +199,18 @@
     def earlier(block, _):
         slot = lax.rem(block, 2)
         fetch(block, slot).wait()
-        fetch(block + 1, 1 - slot).start()
-        prepare_keys(block, slot)
+
+        @pl.when(block + 1 < mine)
+        def _():
+            fetch(block + 1, 1 - slot).start()
+
+        prepare_keys(block, kv_buf.at[slot])
         accumulate(False)
         return 0
 
     lax.fori_loop(0, mine, earlier, 0)
-    slot = lax.rem(mine, 2)
-    fetch(mine, slot).wait()
-    prepare_keys(mine, slot)
+    own_copy.wait()
+    prepare_keys(mine, own_buf)
     accumulate(True)
 
     def finish(step, _):
@@ -214,7 +225,7 @@
     lax.fori_loop(0, rows // step_rows, finish, 0)
 
 
-def attention(q_lat, kv_all, wq, wk, wv, gains, tables):
+def attention(q_lat, kv_all, kv_own, wq, wk, wv, gains, tables):
     rows = q_lat.shape[0]
     heads = wq.shape[1] // LANES
     step_rows = math.gcd(rows, 256)
@@ -222,7 +233,7 @@
     return pl.pallas_call(
         functools.partial(attention_kernel, heads, step_rows),
         out_shape=jax.ShapeDtypeStruct((rows, heads * VDIM), bf16),
-        in_specs=[vm, pl.BlockSpec(memory_space=pl.ANY)] + [vm] * 11,
+        in_specs=[vm, pl.BlockSpec(memory_space=pl.ANY), pl.BlockSpec(memory_space=pl.ANY)] + [vm] * 11,
         out_specs=vm,
         scratch_shapes=[
             pltpu.VMEM((2,) + kv_all.shape[1:], bf16),
@@ -230,10 +241,346 @@
             pltpu.VMEM((heads, LANES, rows), bf16),
             pltpu.VMEM((heads, rows, LANES), bf16),
             pltpu.VMEM((heads, rows, LANES), f32),
+            pltpu.VMEM(kv_own.shape, bf16),
             pltpu.SemaphoreType.DMA((2,)),
+            pltpu.SemaphoreType.DMA,
         ],
         compiler_params=pltpu.CompilerParams(vmem_limit_bytes=48 * 1024 * 1024),
-    )(q_lat, kv_all, wq, wk, wv, *gains, *tables)
+    )(q_lat, kv_all, kv_own, wq, wk, wv, *gains, *tables)
+
+
+MESH = pl.DeviceIdType.MESH
+
+
+def remote(src, dst, send_sem, recv_sem, target):
+    return pltpu.make_async_remote_copy(
+        src_ref=src,
+        dst_ref=dst,
+        send_sem=send_sem,
+        recv_sem=recv_sem,
+        device_id=target,
+        device_id_type=MESH,
+    )
+
+
+def tp_place():
+    me = lax.axis_index("tp")
+    return me, lax.rem(me, 2), lax.div(me, 2)
+
+
+def greet_tp(n_tp, me, barrier):
+    for step in range(1, n_tp):
+        pl.semaphore_signal(
+            barrier, inc=1, device_id={"tp": lax.rem(me + step, n_tp)}, device_id_type=MESH
+        )
+
+
+def tp_gather_kernel(n_tp, x_ref, out_ref, local_sem, own_send, far_send, relay_send, recv):
+    me, core, chip = tp_place()
+    chips = n_tp // 2
+    partner = me + 1 - 2 * core
+    barrier = pltpu.get_barrier_semaphore()
+    greet_tp(n_tp, me, barrier)
+    pl.semaphore_wait(barrier, n_tp - 1)
+    far = []
+    for step in range(1, chips):
+        there = 2 * lax.rem(chip + step, chips) + core
+        copy = remote(x_ref, out_ref.at[me], far_send.at[step - 1], recv.at[me], {"tp": there})
+        copy.start()
+        far.append(copy)
+    near = remote(x_ref, out_ref.at[me], own_send, recv.at[me], {"tp": partner})
+    near.start()
+    keep = pltpu.make_async_copy(x_ref, out_ref.at[me], local_sem)
+    keep.start()
+    relays = []
+    for step in range(1, chips):
+        source = 2 * lax.rem(chip + chips - step, chips) + core
+        remote(x_ref, out_ref.at[source], far_send.at[step - 1], recv.at[source], {"tp": partner}).wait_recv()
+        copy = remote(
+            out_ref.at[source],
+            out_ref.at[source],
+            relay_send.at[step - 1],
+            recv.at[source],
+            {"tp": partner},
+        )
+        copy.start()
+        relays.append(copy)
+    for step in range(chips):
+        source = 2 * lax.rem(chip + step, chips) + 1 - core
+        remote(x_ref, out_ref.at[source], own_send, recv.at[source], {"tp": partner}).wait_recv()
+    for copy in far + relays:
+        copy.wait_send()
+    near.wait_send()
+    keep.wait()
+
+
+def tp_gather(block, identity):
+    n_tp = lax.axis_size("tp")
+    vm = pl.BlockSpec(memory_space=pltpu.VMEM)
+    others = max(1, n_tp // 2 - 1)
+    return pl.pallas_call(
+        functools.partial(tp_gather_kernel, n_tp),
+        out_shape=jax.ShapeDtypeStruct((n_tp,) + block.shape, block.dtype),
+        in_specs=[vm],
+        out_specs=vm,
+        scratch_shapes=[
+            pltpu.SemaphoreType.DMA,
+            pltpu.SemaphoreType.DMA,
+            pltpu.SemaphoreType.DMA((others,)),
+            pltpu.SemaphoreType.DMA((others,)),
+            pltpu.SemaphoreType.DMA((n_tp,)),
+        ],
+        compiler_params=pltpu.CompilerParams(collective_id=identity, has_side_effects=True),
+    )(block)
+
+
+def tp_scatter_kernel(
+    n_tp, x_ref, out_ref, pair_buf, sum_buf, far_buf, pair_send, pair_recv, far_send, far_recv
+):
+    me, core, chip = tp_place()
+    chips = n_tp // 2
+    partner = me + 1 - 2 * core
+    rows = out_ref.shape[0]
+
+    def rows_of(place):
+        return x_ref.at[pl.ds(pl.multiple_of(place * rows, rows), rows), :]
+
+    barrier = pltpu.get_barrier_semaphore()
+    greet_tp(n_tp, me, barrier)
+    pl.semaphore_wait(barrier, n_tp - 1)
+    pairs = []
+    for step in range(1, chips + 1):
+        target_chip = lax.rem(chip + step, chips)
+        copy = remote(
+            rows_of(2 * target_chip + 1 - core),
+            pair_buf.at[step - 1],
+            pair_send.at[step - 1],
+            pair_recv.at[step - 1],
+            {"tp": partner},
+        )
+        copy.start()
+        pairs.append(copy)
+    far = []
+    for step in range(1, chips):
+        there = 2 * lax.rem(chip + step, chips) + core
+        pairs[step - 1].wait_recv()
+        mine = rows_of(there)[...].astype(f32)
+        sum_buf[step - 1] = (mine + pair_buf[step - 1].astype(f32)).astype(bf16)
+        copy = remote(
+            sum_buf.at[step - 1],
+            far_buf.at[step - 1],
+            far_send.at[step - 1],
+            far_recv.at[step - 1],
+            {"tp": there},
+        )
+        copy.start()
+        far.append(copy)
+    pairs[chips - 1].wait_recv()
+    total = rows_of(me)[...].astype(f32) + pair_buf[chips - 1].astype(f32)
+    for step in range(1, chips):
+        far[step - 1].wait_recv()
+        total = total + far_buf[step - 1].astype(f32)
+    out_ref[...] = total.astype(bf16)
+    for copy in pairs + far:
+        copy.wait_send()
+
+
+def tp_scatter(partial, identity):
+    n_tp = lax.axis_size("tp")
+    vm = pl.BlockSpec(memory_space=pltpu.VMEM)
+    chips = n_tp // 2
+    others = max(1, chips - 1)
+    rows, width = partial.shape[0] // n_tp, partial.shape[1]
+    return pl.pallas_call(
+        functools.partial(tp_scatter_kernel, n_tp),
+        out_shape=jax.ShapeDtypeStruct((rows, width), bf16),
+        in_specs=[vm],
+        out_specs=vm,
+        scratch_shapes=[
+            pltpu.VMEM((chips, rows, width), bf16),
+            pltpu.VMEM((others, rows, width), bf16),
+            pltpu.VMEM((others, rows, width), bf16),
+            pltpu.SemaphoreType.DMA((chips,)),
+            pltpu.SemaphoreType.DMA((chips,)),
+            pltpu.SemaphoreType.DMA((others,)),
+            pltpu.SemaphoreType.DMA((others,)),
+        ],
+        compiler_params=pltpu.CompilerParams(
+            collective_id=identity, has_side_effects=True, vmem_limit_bytes=40 * 1024 * 1024
+        ),
+    )(partial)
+
+
+def sp_gather_kernel(
+    n_sp, n_tp, x_ref, out_ref, deep_send, side_send, near_send, far_send, relay_send, recv
+):
+    me, core, chip = tp_place()
+    chips = n_tp // 2
+    partner = me + 1 - 2 * core
+    shard = lax.axis_index("sp")
+    deep, side = lax.div(shard, 2), lax.rem(shard, 2)
+    last_deep = n_sp // 2 - 1
+    rows = x_ref.shape[0] // n_tp
+    other = shard + 1 - 2 * side
+
+    def piece(block, place):
+        return out_ref.at[block, pl.ds(pl.multiple_of(place * rows, rows), rows), :]
+
+    own = x_ref.at[pl.ds(pl.multiple_of(me * rows, rows), rows), :]
+
+    barrier = pltpu.get_barrier_semaphore()
+    greet_tp(n_tp, me, barrier)
+    pl.semaphore_signal(barrier, inc=1, device_id={"sp": other}, device_id_type=MESH)
+
+    @pl.when(deep > 0)
+    def _():
+        pl.semaphore_signal(barrier, inc=1, device_id={"sp": shard - 2}, device_id_type=MESH)
+
+    @pl.when(deep < last_deep)
+    def _():
+        pl.semaphore_signal(barrier, inc=1, device_id={"sp": shard + 2}, device_id_type=MESH)
+
+    neighbours = jnp.minimum(deep, 1) + jnp.minimum(last_deep - deep, 1)
+    pl.semaphore_wait(barrier, n_tp + neighbours)
+
+    def onward(block, source):
+        return remote(source, piece(block, me), deep_send.at[block], recv.at[block, me], {"sp": shard + 2})
+
+    def across(block, source):
+        return remote(source, piece(block, me), side_send.at[block], recv.at[block, me], {"sp": other})
+
+    def near(block):
+        return remote(piece(block, me), piece(block, me), near_send.at[block], recv.at[block, me], {"tp": partner})
+
+    def far(block, step):
+        there = 2 * lax.rem(chip + step, chips) + core
+        return remote(
+            piece(block, me), piece(block, me), far_send.at[block, step - 1], recv.at[block, me], {"tp": there}
+        )
+
+    def relay(block, step):
+        source = 2 * lax.rem(chip + chips - step, chips) + core
+        return remote(
+            piece(block, source),
+            piece(block, source),
+            relay_send.at[block, step - 1],
+            recv.at[block, source],
+            {"tp": partner},
+        )
+
+    def arrived(block, place):
+        remote(
+            piece(block, place), piece(block, place), near_send.at[block], recv.at[block, place], {"tp": partner}
+        ).wait_recv()
+
+    def spread(block):
+        for step in range(1, chips):
+            far(block, step).start()
+        near(block).start()
+
+    def pass_on(block):
+        for step in range(1, chips):
+            arrived(block, 2 * lax.rem(chip + chips - step, chips) + core)
+            relay(block, step).start()
+
+    @pl.when(deep < last_deep)
+    def _():
+        onward(shard, own).start()
+
+    @pl.when(side == 0)
+    def _():
+        across(shard, own).start()
+
+    def receive(k, _):
+        block = shard - 2 * k
+        arrived(block, me)
+
+        @pl.when(deep < last_deep)
+        def _():
+            onward(block, piece(block, me)).start()
+
+        across(block, piece(block, me)).start()
+        spread(block)
+        return 0
+
+    def receive_other(k, _):
+        block = other - 2 * k
+        arrived(block, me)
+        spread(block)
+        return 0
+
+    first_other = 1 - side
+
+    def step(k, _):
+        @pl.when((k > 0) & (k <= deep))
+        def _():
+            receive(k, 0)
+
+        @pl.when((k >= first_other) & (k <= deep))
+        def _():
+            receive_other(k, 0)
+
+        before = k - 1
+
+        @pl.when((before > 0) & (before <= deep))
+        def _():
+            pass_on(shard - 2 * before)
+
+        @pl.when((before >= first_other) & (before <= deep))
+        def _():
+            pass_on(other - 2 * before)
+
+        return 0
+
+    lax.fori_loop(0, deep + 2, step, 0)
+
+    def drain(block, _):
+        for c in range(chips):
+            arrived(block, 2 * c + 1 - core)
+        for s in range(1, chips):
+            far(block, s).wait_send()
+            relay(block, s).wait_send()
+        near(block).wait_send()
+        return 0
+
+    lax.fori_loop(0, shard, drain, 0)
+
+    def drain_sends(k, _):
+        block = shard - 2 * k
+        source = piece(block, me)
+
+        @pl.when(deep < last_deep)
+        def _():
+            onward(block, source).wait_send()
+
+        @pl.when((k > 0) | (side == 0))
+        def _():
+            across(block, source).wait_send()
+
+        return 0
+
+    lax.fori_loop(0, deep + 1, drain_sends, 0)
+
+
+def sp_gather(block, identity):
+    n_sp, n_tp = lax.axis_size("sp"), lax.axis_size("tp")
+    others = max(1, n_tp // 2 - 1)
+    hbm = pl.BlockSpec(memory_space=pl.ANY)
+    return pl.pallas_call(
+        functools.partial(sp_gather_kernel, n_sp, n_tp),
+        out_shape=jax.ShapeDtypeStruct((n_sp,) + block.shape, block.dtype),
+        in_specs=[hbm],
+        out_specs=hbm,
+        scratch_shapes=[
+            pltpu.SemaphoreType.DMA((n_sp,)),
+            pltpu.SemaphoreType.DMA((n_sp,)),
+            pltpu.SemaphoreType.DMA((n_sp,)),
+            pltpu.SemaphoreType.DMA((n_sp, others)),
+            pltpu.SemaphoreType.DMA((n_sp, others)),
+            pltpu.SemaphoreType.DMA((n_sp, n_tp)),
+        ],
+        compiler_params=pltpu.CompilerParams(collective_id=identity, has_side_effects=True),
+    )(block)
 
 
 def local(
@@ -254,7 +601,8 @@
     w_out_pool,
     w_out_attn,
 ):
-    own_input = lax.all_gather(activations, "tp", axis=0, tiled=True)
+    own_input = tp_gather(activations, 0)
+    own_input = own_input.reshape(-1, own_input.shape[-1])
     row_count = own_input.shape[0]
     n_sp = lax.axis_size("sp")
     positions = lax.axis_index("sp") * row_count + jnp.arange(row_count, dtype=jnp.int32)
@@ -264,12 +612,12 @@
     krope_pad = jnp.pad(w_krope, ((0, 0), (NOPE, LANES - HEAD)))
     rope_key = jnp.dot(normed, krope_pad, preferred_element_type=f32).astype(bf16)
     q_width = q_part.shape[1]
-    latents = lax.all_gather(jnp.concatenate([q_part, kv_part], axis=1), "tp", axis=0, tiled=False)
+    latents = tp_gather(jnp.concatenate([q_part, kv_part], axis=1), 1)
     q_lat = jnp.concatenate([latents[i, :, :q_width] for i in range(latents.shape[0])], axis=1)
     kv_lat = jnp.concatenate(
         [latents[i, :, q_width:] for i in range(latents.shape[0])] + [rope_key], axis=1
     )
-    kv_all = lax.all_gather(kv_lat, "sp", axis=0, tiled=False)
+    kv_all = sp_gather(kv_lat, 2)
     pool_in = jnp.dot(normed, w_pool_in, preferred_element_type=f32).astype(bf16)
     prev_rows = from_behind(pool_in[row_count - rim_depth :], "sp", 1)
     extended = jnp.concatenate([prev_rows, pool_in], axis=0)
@@ -278,6 +626,7 @@
     attended = attention(
         q_lat,
         kv_all,
+        kv_lat,
         pad_heads(w_qup, HEAD),
         pad_heads(w_kup, NOPE),
         pad_heads(w_vup, VDIM),
@@ -285,12 +634,8 @@
         rope_tables(row_count, n_sp),
     )
     term = jnp.dot(pool_out, w_out_pool, preferred_element_type=f32)
-    return lax.psum_scatter(
-        (term + jnp.dot(attended, w_out_attn, preferred_element_type=f32)).astype(bf16),
-        "tp",
-        scatter_dimension=0,
-        tiled=True,
-    )
+    attn_term = jnp.dot(attended, w_out_attn, preferred_element_type=f32)
+    return tp_scatter((term + attn_term).astype(bf16), 3)
 
 
 def solution(mesh):

time: 305 us -> 226 us (0.74)
  waiting for transfers between devices: 185 us -> 0.01 us
  Pallas kernels: 56.7 us -> 175 us
  between operations: 13.5 us -> 0.51 us
  local copies, waits for them, and re-layouts: 16.4 us -> 27.4 us
  matrix products: 16 us -> 10.5 us
    all_gather x3 -> x0, waiting for transfers between devices: 146 us -> none  [the longest x1 93.6 us: local(): kv_all = lax.all_gather(kv_lat, 'sp', axis=0, tiled=False)]
    pallas_call x0 -> x4, Pallas kernels: none -> 118 us  [the longest x1 51.1 us: sp_gather(): pl.pallas_call(functools.partial(sp_gather_kernel, n_sp, n_tp), out_shape...]
    reduce_scatter x1 -> x0, waiting for transfers between devices: 38 us -> none  [local(): lax.psum_scatter((term + jnp.dot(attended, w_out_attn, preferred_element_...]
    reshape x3, local copies, waits for them, and re-layouts: 1.5 us -> 6.49 us  [pad_heads(): jnp.pad(shaped, ((0, 0), (0, 0), (0, LANES - width)))]
    unnamed x61 -> x60, local copies, waits for them, and re-layouts: 10.4 us -> 15.3 us
  transfers between devices with their start and end apart: 5 -> 1, of which waited for: 5 -> 0; matrix products, arithmetic and copies ran while one was open for 6% -> 14% of each run, Pallas kernels for 0% -> 57%
where the time goes in v2:
time: 226 us
  Pallas kernels  175 us (77%)
  local copies, waits for them, and re-layouts  27.4 us (12%)
  matrix products  10.5 us (5%)
  other arithmetic  10.4 us (5%)
    pallas_call x1, Pallas kernels, attention(): pl.pallas_call(functools.partial(attention_kernel, heads, step_rows), out...  57.3 us
    pallas_call x1, Pallas kernels, sp_gather(): pl.pallas_call(functools.partial(sp_gather_kernel, n_sp, n_tp), out_shape...  51.1 us
    pallas_call x2, Pallas kernels, tp_gather(): pl.pallas_call(functools.partial(tp_gather_kernel, n_tp), out_shape=jax.S...  44.5 us
    pallas_call x1, Pallas kernels, tp_scatter(): pl.pallas_call(functools.partial(tp_scatter_kernel, n_tp), out_shape=jax....  22.4 us
    unnamed x60, local copies, waits for them, and re-layouts  15.3 us
    reshape x3, local copies, waits for them, and re-layouts, pad_heads(): jnp.pad(shaped, ((0, 0), (0, 0), (0, LANES - width)))  6.49 us
  transfers between devices with their start and end apart: 1, of which 0 were waited for; matrix products, arithmetic and copies ran while one was open for 14% of the time, Pallas kernels for 57%

profile of v2, /device:TPU:30, one launch (start us, length us, event | category | flops | bytes accessed | tf_op | source)
XLA Modules:
  0.0 225.5 jit_solution(3232962949763621610)
XLA Ops:
  0.0 24.7 %shard_map.154 = bf16[4,192,2048]{2,1,0:T(8,128)(2,1)} custom-call(bf16[192,2048]{1,0:T(8,128)(2,1)} %x_ref.1), custom_call_target="tpu_custom_call" | custom-call | tf_op jit(solution)/shard_map/pallas_call | solution.py:321
  24.7 2.6 %multiply_reduce_fusion = f32[4,192]{1,0:T(4,128)S(1)} fusion(bf16[4,192,2048]{2,1,0:T(8,128)(2,1)} %shard_map.154), kind=kLoop, calls=%fused_computation.4 | loop fusion | flops 4717824 | bytes 3148800 | tf_op jit(solution)/shard_map/reduce_sum | solution.py:33
  27.4 2.8 %fusion.1 = bf16[768,2048]{1,0:T(8,128)(2,1)S(1)} fusion(f32[2048]{0:T(1024)S(1)} %copy-done.17, f32[768]{0:T(1024)S(1)} %rsqrt.12, bf16[4,192,2048]{2,1,0:T(8,128)(2,1)} %shard_map.154), kind=kLoop, calls=%fused_computation.2 | loop fusion | flops 6291456 | bytes 6302720 | tf_op jit(solution)/shard_map/convert_element_type | solution.py:609
  32.0 1.4 collective-permute-start
  33.4 1.2 convolution_convert_fusion.1
  34.8 2.9 %convolution_convert_fusion.3 = bf16[768,128]{1,0:T(8,128)(2,1)S(1)} fusion(bf16[768,2048]{1,0:T(8,128)(2,1)} %copy-done.9, bf16[2048,128]{1,0:T(8,128)(2,1)S(1)} %copy-done.23), kind=kOutput, calls=%fused_computation.10 | convolution fusion | flops 402751488 | bytes 3866624 | tf_op jit(solution)/shard_map/dot_general | solution.py:611
  37.7 1.0 pad_maximum_fusion.1.x_ref
  38.7 19.8 %shard_map.155 = bf16[4,768,320]{2,1,0:T(8,128)(2,1)} custom-call(bf16[768,320]{1,0:T(8,128)(2,1)} %pad_maximum_fusion.1.x_ref), custom_call_target="tpu_custom_call" | custom-call | tf_op jit(solution)/shard_map/pallas_call | solution.py:321
  58.6 2.5 %slice_bitcast_fusion.3 = (bf16[768,192]{1,0:T(8,128)(2,1)}, bf16[768,192]{1,0:T(8,128)(2,1)}, bf16[768,192]{1,0:T(8,128)(2,1)}, bf16[768,192]{1,0:T(8,128)(2,1)}) fusion(bf16[4,768,320]{2,1,0:T(8,128)(2,1)} %shard_map.155), kind=kLoop, calls=%fused_computation.33 | loop fusion | bytes 2359296 | tf_op jit(solution)/shard_map/squeeze | solution.py:616
  61.1 1.1 bitcast_dynamic-update-slice_fusion.3
  62.3 1.1 bitcast_dynamic-update-slice_fusion.2
  63.5 1.1 bitcast_dynamic-update-slice_fusion.1
  64.6 1.1 bitcast_dynamic-update-slice_fusion
  65.9 1.4 multiply_sine_fusion
  67.5 3.0 %fusion.2.x_ref.own_ref = bf16[768,640]{1,0:T(8,128)(2,1)S(1)} fusion(bf16[768,640]{1,0:T(8,128)(2,1)S(1)} %bitcast_dynamic-update-slice_fusion, bf16[768,2048]{1,0:T(8,128)(2,1)} %copy-done.9, bf16[2048,32]{0,1:T(8,128)(2,1)S(1)} %copy-done.24), kind=kOutput, calls=%fused_computation.9 | convolution fusion | flops 402751488 | bytes 3473408 | tf_op jit(solution)/shard_map/dot_general | solution.py:613
  70.6 1.4 maximum_maximum_fusion.1
  72.6 51.1 %shard_map.156.kv_ref = bf16[8,768,640]{2,1,0:T(8,128)(2,1)} custom-call(bf16[768,640]{1,0:T(8,128)(2,1)} %copy-done.1), custom_call_target="tpu_custom_call" | custom-call | tf_op jit(solution)/shard_map/pallas_call | solution.py:569
  123.7 1.3 copy.32
  126.0 2.4 %copy.41.wq_ref = bf16[768,512]{1,0:T(8,128)(2,1)} copy(bf16[768,512]{0,1:T(8,128)(2,1)} %bitcast.50) | data formatting | bytes 1572864 | tf_op jit(solution)/shard_map/reshape | solution.py:61
  128.4 1.1 copy.34
  130.3 2.0 copy.42.wk_ref
  132.3 1.1 copy.36
  134.3 2.1 copy.43.wv_ref
  136.4 1.1 copy-done.3
  137.5 1.0 copy-done.4
  138.5 1.0 copy-done.5
  139.6 1.0 copy-done.6
  140.6 1.0 copy-done.7
  141.6 57.3 %shard_map.157 = bf16[768,256]{1,0:T(8,128)(2,1)S(1)} custom-call(bf16[768,768]{1,0:T(8,128)(2,1)S(1)} %pad_maximum_fusion.q_ref, bf16[8,768,640]{2,1,0:T(8,128)(2,1)} %shard_map.156.kv_ref, bf16[768,640]{1,0:T(8,128)(2,1)S(1)} %copy-done.2, bf16[768,512]{1,0:T(8,128)(2,1)S(1)} %copy-done.3, bf16[512,512]{1,0:T(8,128)(2,1)S(1)} %copy-done.4, ...), custom_call_target="tpu_custom_call" | custom-call | tf_op jit(solution)/shard_map/pallas_call | solution.py:233
  199.8 1.4 fusion.9
  201.2 1.0 add_convert_fusion.x_ref
  202.2 22.4 %shard_map.158 = bf16[192,2048]{1,0:T(8,128)(2,1)S(1)} custom-call(bf16[768,2048]{1,0:T(8,128)(2,1)S(1)} %add_convert_fusion.x_ref), custom_call_target="tpu_custom_call" | custom-call | tf_op jit(solution)/shard_map/pallas_call | solution.py:394
  (80 shorter events, 7.3 us)
Async XLA Ops:
  0.0 199.5 %copy-start = (bf16[256,2048]{1,0:T(8,128)(2,1)S(1)}, bf16[256,2048]{1,0:T(8,128)(2,1)}, u32[]{:S(2)}) copy-start(bf16[256,2048]{1,0:T(8,128)(2,1)} %param.30) | copy-start | bytes 3145732
  0.0 27.4 %copy-start.17 = (f32[2048]{0:T(1024)S(1)}, f32[2048]{0:T(1024)}, u32[]{:S(2)}) copy-start(f32[2048]{0:T(1024)} %param.17) | copy-start | bytes 24580
  27.4 2.8 %copy-start.21 = (bf16[2048,256]{1,0:T(8,128)(2,1)S(1)}, bf16[2048,256]{1,0:T(8,128)(2,1)}, u32[]{:S(2)}) copy-start(bf16[2048,256]{1,0:T(8,128)(2,1)} %param.18) | copy-start | bytes 3145732
  30.2 3.2 %copy-start.9 = (bf16[768,2048]{1,0:T(8,128)(2,1)}, bf16[768,2048]{1,0:T(8,128)(2,1)S(1)}, u32[]{:S(2)}) copy-start(bf16[768,2048]{1,0:T(8,128)(2,1)S(1)} %fusion.1) | copy-start | bytes 9437188
  30.2 3.2 %copy-start.22 = (bf16[2048,192]{0,1:T(8,128)(2,1)S(1)}, bf16[2048,192]{0,1:T(8,128)(2,1)}, u32[]{:S(2)}) copy-start(bf16[2048,192]{0,1:T(8,128)(2,1)} %param.20) | copy-start | bytes 2359300
  31.2 0.8 copy-start.10
  31.9 2.9 %copy-start.23 = (bf16[2048,128]{1,0:T(8,128)(2,1)S(1)}, bf16[2048,128]{1,0:T(8,128)(2,1)}, u32[]{:S(2)}) copy-start(bf16[2048,128]{1,0:T(8,128)(2,1)} %param.21) | copy-start | bytes 1572868
  32.0 166.9 %collective-permute-start = (bf16[15,256]{1,0:T(8,128)(2,1)S(1)}, bf16[15,256]{1,0:T(8,128)(2,1)S(1)}, u32[]{:S(2)}, u32[]{:S(2)}) collective-permute-start(bf16[15,256]{1,0:T(8,128)(2,1)S(1)} %slice.72), channel_id=1, source_target_pairs={{0,4},{4,8},{8,12},{12,16},{16,20},{20,24},{24,28},{1,5},{5,9},{9,... | collective-permute-start | bytes 23048 | tf_op jit(solution)/shard_map/ppermute | solution.py:28
  58.5 8.9 %copy-start.24 = (bf16[2048,32]{0,1:T(8,128)(2,1)S(1)}, bf16[2048,32]{0,1:T(8,128)(2,1)}, u32[]{:S(2)}) copy-start(bf16[2048,32]{0,1:T(8,128)(2,1)} %param.22) | copy-start | bytes 393220
  67.5 4.6 %copy-start.19 = (f32[96]{0:T(128)S(1)}, f32[96]{0:T(128)}, u32[]{:S(2)}) copy-start(f32[96]{0:T(128)} %param.29) | copy-start | bytes 1156
  67.5 4.5 %copy-start.20 = (f32[96]{0:T(128)S(1)}, f32[96]{0:T(128)}, u32[]{:S(2)}) copy-start(f32[96]{0:T(128)} %param.28) | copy-start | bytes 1156
  67.5 4.5 %copy-start.12 = (bf16[768,192]{1,0:T(8,128)(2,1)S(1)}, bf16[768,192]{1,0:T(8,128)(2,1)}, u32[]{:S(2)}) copy-start(bf16[768,192]{1,0:T(8,128)(2,1)} %get-tuple-element.5) | copy-start | bytes 884740
  67.5 4.5 %copy-start.13 = (bf16[768,192]{1,0:T(8,128)(2,1)S(1)}, bf16[768,192]{1,0:T(8,128)(2,1)}, u32[]{:S(2)}) copy-start(bf16[768,192]{1,0:T(8,128)(2,1)} %get-tuple-element.6) | copy-start | bytes 884740
  67.5 4.5 %copy-start.14 = (bf16[768,192]{1,0:T(8,128)(2,1)S(1)}, bf16[768,192]{1,0:T(8,128)(2,1)}, u32[]{:S(2)}) copy-start(bf16[768,192]{1,0:T(8,128)(2,1)} %get-tuple-element.7) | copy-start | bytes 884740
  67.5 4.5 %copy-start.15 = (bf16[768,192]{1,0:T(8,128)(2,1)S(1)}, bf16[768,192]{1,0:T(8,128)(2,1)}, u32[]{:S(2)}) copy-start(bf16[768,192]{1,0:T(8,128)(2,1)} %get-tuple-element.8) | copy-start | bytes 884740
  70.6 2.0 copy-start.1
  126.0 10.4 %copy-start.18 = (f32[768]{0:T(1024)S(1)}, f32[768]{0:T(1024)}, u32[]{:S(2)}) copy-start(f32[768]{0:T(1024)} %param.23) | copy-start | bytes 9220
  126.0 10.4 %copy-start.2 = (bf16[768,640]{1,0:T(8,128)(2,1)S(1)}, bf16[768,640]{1,0:T(8,128)(2,1)}, u32[]{:S(2)}) copy-start(bf16[768,640]{1,0:T(8,128)(2,1)} %copy-done.1) | copy-start | bytes 2949124
  126.0 10.4 %copy-start.8 = (f32[512]{0:T(512)S(1)}, f32[512]{0:T(512)}, u32[]{:S(2)}) copy-start(f32[512]{0:T(512)} %param.24) | copy-start | bytes 6148
  136.3 1.1 copy-start.3
  137.5 1.0 copy-start.4
  138.5 1.0 copy-start.5
  139.6 1.0 copy-start.6
  140.6 1.0 copy-start.7
  141.6 57.3 %copy-start.11 = (bf16[768,256]{1,0:T(8,128)(2,1)S(1)}, bf16[768,256]{1,0:T(8,128)(2,1)}, u32[]{:S(2)}) copy-start(bf16[768,256]{1,0:T(8,128)(2,1)} %copy-done.10) | copy-start | bytes 1179652
  199.2 0.7 copy-start.25
  199.8 1.4 copy-start.16

commit v3 on v2

--- a/solution.py
+++ b/solution.py
@@ -54,11 +54,12 @@
     return window_sum / divisor - as_float[rim_depth:]
 
 
-def pad_heads(weight, width):
-    depth = weight.shape[0]
-    heads = weight.shape[1] // width
-    shaped = weight.reshape(depth, heads, width)
-    return jnp.pad(shaped, ((0, 0), (0, 0), (0, LANES - width))).reshape(depth, heads * LANES)
+def pad_heads(weight_ref, padded_ref, width):
+    weight = weight_ref[...].astype(f32)
+    padded_ref[...] = jnp.zeros_like(padded_ref)
+    for h in range(weight.shape[1] // width):
+        head = weight[:, h * width : (h + 1) * width]
+        padded_ref[:, h * LANES : h * LANES + width] = head.astype(bf16)
 
 
 def pad_row(gain):
@@ -102,9 +103,9 @@
     q_ref,
     kv_ref,
     own_ref,
-    wq_ref,
-    wk_ref,
-    wv_ref,
+    wq_raw,
+    wk_raw,
+    wv_raw,
     qlat_gain,
     kvlat_gain,
     qh_gain,
@@ -120,6 +121,9 @@
     values,
     acc,
     own_buf,
+    wq_ref,
+    wk_ref,
+    wv_ref,
     sem,
     own_sem,
 ):
@@ -138,6 +142,10 @@
     @pl.when(mine > 0)
     def _():
         fetch(0, 0).start()
+
+    pad_heads(wq_raw, wq_ref, HEAD)
+    pad_heads(wk_raw, wk_ref, NOPE)
+    pad_heads(wv_raw, wv_ref, VDIM)
 
     def angles(block, at):
         cr, sr = cos_r[at, :], sin_r[at, :]
@@ -227,7 +235,7 @@
 
 def attention(q_lat, kv_all, kv_own, wq, wk, wv, gains, tables):
     rows = q_lat.shape[0]
-    heads = wq.shape[1] // LANES
+    heads = wq.shape[1] // HEAD
     step_rows = math.gcd(rows, 256)
     vm = pl.BlockSpec(memory_space=pltpu.VMEM)
     return pl.pallas_call(
@@ -242,6 +250,9 @@
             pltpu.VMEM((heads, rows, LANES), bf16),
             pltpu.VMEM((heads, rows, LANES), f32),
             pltpu.VMEM(kv_own.shape, bf16),
+            pltpu.VMEM((wq.shape[0], heads * LANES), bf16),
+            pltpu.VMEM((wk.shape[0], heads * LANES), bf16),
+            pltpu.VMEM((wv.shape[0], heads * LANES), bf16),
             pltpu.SemaphoreType.DMA((2,)),
             pltpu.SemaphoreType.DMA,
         ],
@@ -627,9 +638,9 @@
         q_lat,
         kv_all,
         kv_lat,
-        pad_heads(w_qup, HEAD),
-        pad_heads(w_kup, NOPE),
-        pad_heads(w_vup, VDIM),
+        w_qup,
+        w_kup,
+        w_vup,
         (qlat_gain.reshape(1, -1), kvlat_gain.reshape(1, -1), pad_row(qhead_gain), pad_row(khead_gain)),
         rope_tables(row_count, n_sp),
     )

time: 226 us -> 214 us (0.947)
  local copies, waits for them, and re-layouts: 27.4 us -> 14.8 us
    reshape x3 -> x0, local copies, waits for them, and re-layouts: 6.49 us -> none  [pad_heads(): jnp.pad(shaped, ((0, 0), (0, 0), (0, LANES - width)))]
    unnamed x60 -> x57, local copies, waits for them, and re-layouts: 15.3 us -> 11.9 us
    pad x3 -> x0, local copies, waits for them, and re-layouts: 2.6 us -> none  [pad_heads(): jnp.pad(shaped, ((0, 0), (0, 0), (0, LANES - width)))]
  transfers between devices with their start and end apart: 1 -> 1, of which waited for: 0 -> 0; matrix products, arithmetic and copies ran while one was open for 14% -> 9% of each run, Pallas kernels for 57% -> 60%
where the time goes in v3:
time: 214 us; the launch traced here: 213 us
  Pallas kernels  175 us (82%)
  local copies, waits for them, and re-layouts  14.8 us (7%)
  matrix products  10.5 us (5%)
  other arithmetic  10.4 us (5%)
    pallas_call x1, Pallas kernels, attention(): pl.pallas_call(functools.partial(attention_kernel, heads, step_rows), out...  57.3 us
    pallas_call x1, Pallas kernels, sp_gather(): pl.pallas_call(functools.partial(sp_gather_kernel, n_sp, n_tp), out_shape...  51.1 us
    pallas_call x2, Pallas kernels, tp_gather(): pl.pallas_call(functools.partial(tp_gather_kernel, n_tp), out_shape=jax.S...  44.5 us
    pallas_call x1, Pallas kernels, tp_scatter(): pl.pallas_call(functools.partial(tp_scatter_kernel, n_tp), out_shape=jax....  22.4 us
    unnamed x57, local copies, waits for them, and re-layouts  11.9 us
  transfers between devices with their start and end apart: 1, of which 0 were waited for; matrix products, arithmetic and copies ran while one was open for 9% of the time, Pallas kernels for 60%

profile of v3, /device:TPU:30, one launch (start us, length us, event | category | flops | bytes accessed | tf_op | source)
XLA Modules:
  0.0 212.9 jit_solution(9693354098325833766)
XLA Ops:
  0.0 24.7 %shard_map.154 = bf16[4,192,2048]{2,1,0:T(8,128)(2,1)} custom-call(bf16[192,2048]{1,0:T(8,128)(2,1)} %x_ref.1), custom_call_target="tpu_custom_call" | custom-call | tf_op jit(solution)/shard_map/pallas_call | solution.py:332
  24.7 2.6 %multiply_reduce_fusion = f32[4,192]{1,0:T(4,128)S(1)} fusion(bf16[4,192,2048]{2,1,0:T(8,128)(2,1)} %shard_map.154), kind=kLoop, calls=%fused_computation.4 | loop fusion | flops 4717824 | bytes 3148800 | tf_op jit(solution)/shard_map/reduce_sum | solution.py:33
  27.4 2.8 %fusion.1 = bf16[768,2048]{1,0:T(8,128)(2,1)S(1)} fusion(f32[2048]{0:T(1024)S(1)} %copy-done.17, f32[768]{0:T(1024)S(1)} %rsqrt.12, bf16[4,192,2048]{2,1,0:T(8,128)(2,1)} %shard_map.154), kind=kLoop, calls=%fused_computation.2 | loop fusion | flops 6291456 | bytes 6302720 | tf_op jit(solution)/shard_map/convert_element_type | solution.py:620
  30.2 1.0 convolution_convert_fusion
  31.2 0.7 copy-done.10
  31.9 1.4 collective-permute-start
  33.4 1.2 convolution_convert_fusion.1
  34.6 0.2 copy.21
  34.8 2.9 %convolution_convert_fusion.3 = bf16[768,128]{1,0:T(8,128)(2,1)S(1)} fusion(bf16[768,2048]{1,0:T(8,128)(2,1)} %copy-done.9, bf16[2048,128]{1,0:T(8,128)(2,1)S(1)} %copy-done.23), kind=kOutput, calls=%fused_computation.10 | convolution fusion | flops 402751488 | bytes 3866624 | tf_op jit(solution)/shard_map/dot_general | solution.py:622
  37.7 1.0 pad_maximum_fusion.1.x_ref
  38.7 19.8 %shard_map.155 = bf16[4,768,320]{2,1,0:T(8,128)(2,1)} custom-call(bf16[768,320]{1,0:T(8,128)(2,1)} %pad_maximum_fusion.1.x_ref), custom_call_target="tpu_custom_call" | custom-call | tf_op jit(solution)/shard_map/pallas_call | solution.py:332
  58.6 2.6 %slice_bitcast_fusion.3 = (bf16[768,192]{1,0:T(8,128)(2,1)}, bf16[768,192]{1,0:T(8,128)(2,1)}, bf16[768,192]{1,0:T(8,128)(2,1)}, bf16[768,192]{1,0:T(8,128)(2,1)}) fusion(bf16[4,768,320]{2,1,0:T(8,128)(2,1)} %shard_map.155), kind=kLoop, calls=%fused_computation.33 | loop fusion | bytes 2359296 | tf_op jit(solution)/shard_map/squeeze | solution.py:627
  61.1 1.1 bitcast_dynamic-update-slice_fusion.3
  62.3 1.1 bitcast_dynamic-update-slice_fusion.2
  63.5 1.1 bitcast_dynamic-update-slice_fusion.1
  64.6 1.1 bitcast_dynamic-update-slice_fusion
  65.9 1.4 multiply_sine_fusion
  67.5 3.0 %fusion.2.x_ref.own_ref = bf16[768,640]{1,0:T(8,128)(2,1)S(1)} fusion(bf16[768,640]{1,0:T(8,128)(2,1)S(1)} %bitcast_dynamic-update-slice_fusion, bf16[768,2048]{1,0:T(8,128)(2,1)} %copy-done.9, bf16[2048,32]{0,1:T(8,128)(2,1)S(1)} %copy-done.24), kind=kOutput, calls=%fused_computation.9 | convolution fusion | flops 402751488 | bytes 3473408 | tf_op jit(solution)/shard_map/dot_general | solution.py:624
  70.6 1.3 maximum_maximum_fusion.1
  72.1 0.5 pad_maximum_fusion.q_ref
  72.7 51.1 %shard_map.156.kv_ref = bf16[8,768,640]{2,1,0:T(8,128)(2,1)} custom-call(bf16[768,640]{1,0:T(8,128)(2,1)} %copy-done.1), custom_call_target="tpu_custom_call" | custom-call | tf_op jit(solution)/shard_map/pallas_call | solution.py:580
  123.8 1.2 copy-done.2
  125.0 1.0 copy-done.3
  126.0 1.0 copy-done.4
  127.0 1.1 copy-done.5
  128.1 0.9 copy-done.7
  129.0 57.3 %shard_map.157 = bf16[768,256]{1,0:T(8,128)(2,1)S(1)} custom-call(bf16[768,768]{1,0:T(8,128)(2,1)S(1)} %pad_maximum_fusion.q_ref, bf16[8,768,640]{2,1,0:T(8,128)(2,1)} %shard_map.156.kv_ref, bf16[768,640]{1,0:T(8,128)(2,1)S(1)} %copy-done.2, bf16[768,384]{1,0:T(8,128)(2,1)S(1)} %copy-done.5, bf16[512,256]{1,0:T(8,128)(2,1)S(1)} %copy-done.6, ...), custom_call_target="tpu_custom_call" | custom-call | tf_op jit(solution)/shard_map/pallas_call | solution.py:241
  186.9 0.4 copy-done.25
  187.3 1.4 fusion.9
  188.7 1.0 add_convert_fusion.x_ref
  189.7 22.4 %shard_map.158 = bf16[192,2048]{1,0:T(8,128)(2,1)S(1)} custom-call(bf16[768,2048]{1,0:T(8,128)(2,1)S(1)} %add_convert_fusion.x_ref), custom_call_target="tpu_custom_call" | custom-call | tf_op jit(solution)/shard_map/pallas_call | solution.py:405
  212.1 0.9 copy.31
  (71 shorter events, 1.1 us)
Async XLA Ops:
  0.0 186.9 %copy-start = (bf16[256,2048]{1,0:T(8,128)(2,1)S(1)}, bf16[256,2048]{1,0:T(8,128)(2,1)}, u32[]{:S(2)}) copy-start(bf16[256,2048]{1,0:T(8,128)(2,1)} %param.30) | copy-start | bytes 3145732
  0.0 27.4 %copy-start.17 = (f32[2048]{0:T(1024)S(1)}, f32[2048]{0:T(1024)}, u32[]{:S(2)}) copy-start(f32[2048]{0:T(1024)} %param.17) | copy-start | bytes 24580
  27.4 2.8 %copy-start.21 = (bf16[2048,256]{1,0:T(8,128)(2,1)S(1)}, bf16[2048,256]{1,0:T(8,128)(2,1)}, u32[]{:S(2)}) copy-start(bf16[2048,256]{1,0:T(8,128)(2,1)} %param.18) | copy-start | bytes 3145732
  30.2 3.2 %copy-start.9 = (bf16[768,2048]{1,0:T(8,128)(2,1)}, bf16[768,2048]{1,0:T(8,128)(2,1)S(1)}, u32[]{:S(2)}) copy-start(bf16[768,2048]{1,0:T(8,128)(2,1)S(1)} %fusion.1) | copy-start | bytes 9437188
  30.2 3.2 %copy-start.22 = (bf16[2048,192]{0,1:T(8,128)(2,1)S(1)}, bf16[2048,192]{0,1:T(8,128)(2,1)}, u32[]{:S(2)}) copy-start(bf16[2048,192]{0,1:T(8,128)(2,1)} %param.20) | copy-start | bytes 2359300
  31.2 0.8 copy-start.10
  31.9 2.9 %copy-start.23 = (bf16[2048,128]{1,0:T(8,128)(2,1)S(1)}, bf16[2048,128]{1,0:T(8,128)(2,1)}, u32[]{:S(2)}) copy-start(bf16[2048,128]{1,0:T(8,128)(2,1)} %param.21) | copy-start | bytes 1572868
  31.9 154.4 %collective-permute-start = (bf16[15,256]{1,0:T(8,128)(2,1)S(1)}, bf16[15,256]{1,0:T(8,128)(2,1)S(1)}, u32[]{:S(2)}, u32[]{:S(2)}) collective-permute-start(bf16[15,256]{1,0:T(8,128)(2,1)S(1)} %slice.72), channel_id=1, source_target_pairs={{0,4},{4,8},{8,12},{12,16},{16,20},{20,24},{24,28},{1,5},{5,9},{9,... | collective-permute-start | bytes 23048 | tf_op jit(solution)/shard_map/ppermute | solution.py:28
  58.5 8.9 %copy-start.24 = (bf16[2048,32]{0,1:T(8,128)(2,1)S(1)}, bf16[2048,32]{0,1:T(8,128)(2,1)}, u32[]{:S(2)}) copy-start(bf16[2048,32]{0,1:T(8,128)(2,1)} %param.22) | copy-start | bytes 393220
  67.5 4.5 %copy-start.19 = (f32[96]{0:T(128)S(1)}, f32[96]{0:T(128)}, u32[]{:S(2)}) copy-start(f32[96]{0:T(128)} %param.29) | copy-start | bytes 1156
  67.5 4.5 %copy-start.20 = (f32[96]{0:T(128)S(1)}, f32[96]{0:T(128)}, u32[]{:S(2)}) copy-start(f32[96]{0:T(128)} %param.28) | copy-start | bytes 1156
  67.5 4.5 %copy-start.12 = (bf16[768,192]{1,0:T(8,128)(2,1)S(1)}, bf16[768,192]{1,0:T(8,128)(2,1)}, u32[]{:S(2)}) copy-start(bf16[768,192]{1,0:T(8,128)(2,1)} %get-tuple-element.5) | copy-start | bytes 884740
  67.5 4.5 %copy-start.13 = (bf16[768,192]{1,0:T(8,128)(2,1)S(1)}, bf16[768,192]{1,0:T(8,128)(2,1)}, u32[]{:S(2)}) copy-start(bf16[768,192]{1,0:T(8,128)(2,1)} %get-tuple-element.6) | copy-start | bytes 884740
  67.5 4.5 %copy-start.14 = (bf16[768,192]{1,0:T(8,128)(2,1)S(1)}, bf16[768,192]{1,0:T(8,128)(2,1)}, u32[]{:S(2)}) copy-start(bf16[768,192]{1,0:T(8,128)(2,1)} %get-tuple-element.7) | copy-start | bytes 884740
  67.5 4.5 %copy-start.15 = (bf16[768,192]{1,0:T(8,128)(2,1)S(1)}, bf16[768,192]{1,0:T(8,128)(2,1)}, u32[]{:S(2)}) copy-start(bf16[768,192]{1,0:T(8,128)(2,1)} %get-tuple-element.8) | copy-start | bytes 884740
  70.6 2.0 copy-start.1
  72.6 51.1 %copy-start.18 = (f32[768]{0:T(1024)S(1)}, f32[768]{0:T(1024)}, u32[]{:S(2)}) copy-start(f32[768]{0:T(1024)} %param.23) | copy-start | bytes 9220
  72.6 51.1 %copy-start.6 = (bf16[512,256]{1,0:T(8,128)(2,1)S(1)}, bf16[512,256]{1,0:T(8,128)(2,1)}, u32[]{:S(2)}) copy-start(bf16[512,256]{1,0:T(8,128)(2,1)} %wk_raw.1) | copy-start | bytes 786436
  72.6 51.1 %copy-start.8 = (f32[512]{0:T(512)S(1)}, f32[512]{0:T(512)}, u32[]{:S(2)}) copy-start(f32[512]{0:T(512)} %param.24) | copy-start | bytes 6148
  123.8 1.2 copy-start.2
  125.0 1.0 copy-start.3
  126.0 1.0 copy-start.4
  127.0 1.1 copy-start.5
  128.1 0.9 copy-start.7
  129.0 57.3 %copy-start.11 = (bf16[768,256]{1,0:T(8,128)(2,1)S(1)}, bf16[768,256]{1,0:T(8,128)(2,1)}, u32[]{:S(2)}) copy-start(bf16[768,256]{1,0:T(8,128)(2,1)} %copy-done.10) | copy-start | bytes 1179652
  186.6 0.7 copy-start.25
  187.3 1.4 copy-start.16
